TPU v7x, 128 devices: a whole 4x4x4 slice. The times are simulated.
128 devices in a mesh: kv: 16 (over z, y), tp: 8 (over x, core).
Axes of the slice: x: 4, y: 4, z: 4, core: 2. Of those that a mesh axis runs over, the one named last changes fastest.
Arguments:
- tokens: bfloat16 [32, 4096], P(None, 'kv'), may hold values from -40 to 40, as said below
- norm_gain: float32 [4096], P('kv'), may hold values from 0.1 to 1.9
- w_query: bfloat16 [4096, 2048], P('kv', 'tp'), may hold values from -0.09375 to 0.09375
- w_key: bfloat16 [4096, 512], P('kv', 'tp'), may hold values from -0.09375 to 0.09375
- w_value: bfloat16 [4096, 512], P('kv', 'tp'), may hold values from -0.09375 to 0.09375
- forget_weight: bfloat16 [4096, 32], replicated, may hold values from -0.09375 to 0.09375
- forget_bias: float32 [32], P('tp'), may hold values from -1 to 3
- kv_cache: bfloat16 [32, 20480, 8, 128], P(None, 'kv', 'tp'), may hold values from -6 to 6
- cum_gates: float32 [32, 32, 20480], P(None, 'tp', 'kv'), may hold values from -20740 to 0, as said below
- lengths: int32 [32], replicated, may hold values from 1 to 20480, as said below
- w_out: bfloat16 [2048, 4096], P('tp', 'kv'), may hold values from -0.25 to 0.25
Outputs:
- mixed: bfloat16 [32, 4096], P(None, 'kv')
- log_weight: float32 [32, 32], P(None, 'tp')
Inputs may be any that keep to these rules, and one draw needn't show every extreme that they name: Columns of tokens come in 16 groups of equal width. `cum_gates`: each row does not rise along the positions. `lengths`: some sequence has all 20480 positions cached.
All inputs are finite; a program needn't handle non-finite values.
Results may differ from a plain program's by a relative error of at most 0.0307.
Values may be sent and summed in bfloat16 or wider, within the bound.
A program may use at most 64 MiB of HBM per device.

v0:
```python
import jax
import jax.numpy as jnp
from jax import lax
from jax.sharding import Mesh
from jax.sharding import PartitionSpec as P

KV = ("kv_0", "kv_1")


norm_eps = 1e-05
masked_floor = -1e30


def by_axis(array, axes):
    for axis in axes:
        array = lax.psum(array, axis)
    return array


def sent_to_all(array, axis):
    copies = jnp.broadcast_to(array, (lax.axis_size(axis), *array.shape))
    return lax.all_to_all(copies, axis, split_axis=0, concat_axis=0, tiled=True)


def gathered_once(array, axis):
    leaves = jax.tree.leaves(array)
    turns = sorted(range(len(leaves)), key=lambda k: -leaves[k].size)
    width = (1, *leaves[turns[0]].shape)[-1]
    lines = [
        jnp.pad(leaves[k].reshape(-1), (0, -leaves[k].size % width)).reshape(-1, width)
        for k in turns
    ]
    both, at, found = (sent_to_all(jnp.concatenate(lines), axis), 0, {})
    for k, line in zip(turns, lines):
        slab = both[:, at : at + len(line)].reshape(len(both), -1)
        found[k] = slab[:, : leaves[k].size].reshape(-1, *leaves[k].shape)
        at += len(line)
    numbers = iter(range(len(leaves)))
    return jax.tree.map(lambda _: found[next(numbers)], array)


def combined_pairwise(pieces, combine):
    while len(jax.tree.leaves(pieces)[0]) > 1:
        pieces = jax.vmap(combine)(
            *(jax.tree.map(lambda part: part[side::2], pieces) for side in (0, 1))
        )
    return jax.tree.map(lambda part: part[0], pieces)


def combined_all(array, axis, combine):
    pieces = gathered_once(array, axis)
    return combined_pairwise(pieces, combine)


def taken_together(array, axis):
    return sent_to_all(array, axis).astype(jnp.float32).sum(axis=0)


def finish_rows(row_squares, sum_query, sum_keyval, sum_gate, forget_bias, model_width):
    row_scale = lax.rsqrt(row_squares / model_width + norm_eps)[:, None]
    query = (row_scale * sum_query).astype(jnp.bfloat16)
    keyval = (row_scale * sum_keyval).astype(jnp.bfloat16)
    log_gate = jax.nn.log_sigmoid(row_scale * sum_gate + forget_bias)
    return (query, keyval, log_gate)


def combine_parts(first_part, second_part):
    peak_one, sum_one, vals_one, anchor_one = first_part
    peak_two, sum_two, vals_two, anchor_two = second_part
    peak = jnp.maximum(peak_one, peak_two)
    factor_one = jnp.exp(peak_one - peak)
    factor_two = jnp.exp(peak_two - peak)
    return (
        peak,
        sum_one * factor_one + sum_two * factor_two,
        vals_one * factor_one[..., None] + vals_two * factor_two[..., None],
        anchor_one + anchor_two,
    )


def shards(
    tokens,
    norm_gain,
    w_query,
    w_key,
    w_value,
    forget_weight,
    forget_bias,
    kv_cache,
    cum_gates,
    lengths,
    w_out,
):
    rows_count, col_count = tokens.shape
    span_len = kv_cache.shape[1]
    kv_local = kv_cache.shape[2]
    head_size = kv_cache.shape[3] // 2
    heads_local = cum_gates.shape[1]
    group_size = heads_local // kv_local
    model_width = col_count * lax.axis_size(KV)
    tokens_f = tokens.astype(jnp.float32)
    squares = jnp.sum(tokens_f * tokens_f, axis=1)
    normalized_input = (tokens_f * norm_gain).astype(jnp.bfloat16)
    gate_cols = lax.dynamic_slice(
        forget_weight,
        (lax.axis_index(KV) * col_count, lax.axis_index("tp") * heads_local),
        (col_count, heads_local),
    )
    part_query = jnp.dot(normalized_input, w_query, preferred_element_type=jnp.float32)
    part_keyval = jnp.concatenate(
        [
            jnp.dot(normalized_input, w_key, preferred_element_type=jnp.float32),
            jnp.dot(normalized_input, w_value, preferred_element_type=jnp.float32),
        ],
        axis=1,
    )
    part_gate = jnp.dot(normalized_input, gate_cols, preferred_element_type=jnp.float32)
    total_sq, sum_query, sum_keyval, sum_gate = (
        by_axis(squares.astype(jnp.bfloat16), KV).astype(jnp.float32),
        by_axis(part_query.astype(jnp.bfloat16), KV).astype(jnp.float32),
        by_axis(part_keyval.astype(jnp.bfloat16), KV).astype(jnp.float32),
        by_axis(part_gate.astype(jnp.bfloat16), KV).astype(jnp.float32),
    )
    query, keyval, log_gate = finish_rows(
        total_sq, sum_query, sum_keyval, sum_gate, forget_bias, model_width
    )
    inv_root = head_size ** (-0.5)
    query_head_rows = query.reshape(rows_count, kv_local, group_size, head_size)
    cached_keys = kv_cache[:, :, :, :head_size]
    cached_vals = kv_cache[:, :, :, head_size:]
    scores = (
        jnp.einsum(
            "bkgd,blkd->bkgl", query_head_rows, cached_keys, preferred_element_type=jnp.float32
        )
        * inv_root
    )
    biased = scores - cum_gates.reshape(rows_count, kv_local, group_size, span_len)
    first_pos = lax.axis_index(KV) * span_len
    positions = first_pos + lax.iota(jnp.int32, span_len)
    in_range = positions[None, :] < lengths[:, None]
    last_pos = lengths - 1
    holds_last = (last_pos >= first_pos) & (last_pos < first_pos + span_len)
    last_index = jnp.clip(last_pos - first_pos, 0, span_len - 1)
    last_cum = jnp.take_along_axis(
        cum_gates, jnp.broadcast_to(last_index[:, None, None], (rows_count, heads_local, 1)), axis=2
    )[:, :, 0]
    cum_query = last_cum + log_gate
    fresh_key_row = keyval[:, : kv_local * head_size].reshape(rows_count, kv_local, head_size)
    value_new = keyval[:, kv_local * head_size :].reshape(rows_count, kv_local, head_size)
    new_biased = (
        jnp.einsum(
            "pnof,pnf->pno", query_head_rows, fresh_key_row, preferred_element_type=jnp.float32
        )
        * inv_root
    )
    new_biased = new_biased - cum_query.reshape(rows_count, kv_local, group_size)
    range_mask = in_range[:, None, None, :]
    owner_mask = holds_last[:, None, None]
    peak_local = jnp.max(jnp.where(range_mask, biased, masked_floor), axis=-1)
    peak_local = jnp.where(owner_mask, jnp.maximum(peak_local, new_biased), peak_local)
    weights = jnp.where(range_mask, jnp.exp(biased - peak_local[..., None]), 0.0)
    new_weight = jnp.where(owner_mask, jnp.exp(new_biased - peak_local), 0.0)
    weight_sum = jnp.sum(weights, axis=-1) + new_weight
    weighted = jnp.einsum(
        "bkgl,blkd->bkgd",
        weights.astype(jnp.bfloat16),
        cached_vals,
        preferred_element_type=jnp.float32,
    )
    weighted = (
        weighted
        + new_weight.astype(jnp.bfloat16).astype(jnp.float32)[..., None]
        * value_new.astype(jnp.float32)[:, :, None, :]
    )
    anchor = jnp.where(holds_last[:, None], cum_query, 0.0).reshape(
        rows_count, kv_local, group_size
    )
    peak, weight_sum, weighted, anchor = combined_all(
        (peak_local, weight_sum, weighted, anchor), KV, combine_parts
    )
    attended = (
        (weighted / weight_sum[..., None])
        .astype(jnp.bfloat16)
        .reshape(rows_count, heads_local * head_size)
    )
    log_weight = (peak + jnp.log(weight_sum) + anchor).reshape(rows_count, heads_local)
    part_out = jnp.dot(attended, w_out, preferred_element_type=jnp.float32)
    mixed = (
        taken_together(part_out.astype(jnp.bfloat16), "tp").astype(jnp.float32).astype(jnp.bfloat16)
    )
    return (mixed, log_weight)


def solution(mesh):
    torus = Mesh(mesh.devices.reshape(4, 4, mesh.shape["tp"]), ("kv_0", "kv_1", "tp"))
    placed = (
        P(None, KV),
        P(KV),
        P(KV, "tp"),
        P(KV, "tp"),
        P(KV, "tp"),
        P(),
        P("tp"),
        P(None, KV, "tp", None),
        P(None, "tp", KV),
        P(),
        P("tp", KV),
    )
    return jax.shard_map(
        shards, mesh=torus, in_specs=placed, out_specs=(P(None, KV), P(None, "tp")), check_vma=False
    )
```

profile of v0, /device:TPU:1, one launch (start us, length us, event | category | flops | bytes accessed | tf_op | source)
XLA Modules:
  0.0 102.7 jit_solution(4560520956044450282)
XLA Ops:
  0.7 0.9 fusion.23
  1.6 0.9 convolution_convert_fusion.2
  2.5 0.9 convolution_convert_fusion.3
  3.4 1.1 %convolution_convert_fusion.1 = bf16[32,256]{1,0:T(8,128)(2,1)S(1)} fusion(bf16[256,256]{1,0:T(8,128)(2,1)} %param.13, bf16[32,256]{1,0:T(8,128)(2,1)} %param.11, f32[256]{0:T(256)} %param.12), kind=kOutput, calls=%fused_computation.11 | convolution fusion | flops 4227072 | bytes 164864 | tf_op jit(solution)/shard_map/dot_general | solution.py:109
  4.6 0.9 convolution_convert_fusion.4
  5.5 15.4 %all-reduce.1 = (bf16[32,4]{0,1:T(4,128)(2,1)S(1)}, bf16[32]{0:T(256)(128)(2,1)S(1)}, bf16[32,256]{1,0:T(8,128)(2,1)S(1)}, bf16[32,128]{1,0:T(8,128)(2,1)S(1)}) all-reduce(bf16[32,4]{0,1:T(4,128)(2,1)S(1)} %convolution_convert_fusion.4, bf16[32]{0:T(256)(128)(2,1)S(1)} %fusion.23, ...), channel_id=1, replica_groups=mesh['kv_0'=4,'kv_1'=4,'tp'=8] {'kv_0'}, use_global_device_ids=true, to_apply=%region_8.0 | all-reduce | flops 12448 | bytes 49792 | tf_op jit(solution)/shard_map/psum | solution.py:16
  20.9 13.6 %all-reduce = (bf16[32,4]{0,1:T(4,128)(2,1)S(1)}, bf16[32]{0:T(256)(128)(2,1)S(1)}, bf16[32,256]{1,0:T(8,128)(2,1)S(1)}, bf16[32,128]{1,0:T(8,128)(2,1)S(1)}) all-reduce(bf16[32,4]{0,1:T(4,128)(2,1)S(1)} %get-tuple-element.6, bf16[32]{0:T(256)(128)(2,1)S(1)} %get-tuple-element.7, ...), channel_id=1, replica_groups=mesh['kv_0'=4,'kv_1'=4,'tp'=8] {'kv_1'}, use_global_device_ids=true, to_apply=%region_9.10 | all-reduce | flops 12448 | bytes 49792 | tf_op jit(solution)/shard_map/psum | solution.py:16
  34.7 0.8 broadcast_compare_fusion
  35.4 7.0 %select_reduce_fusion = (f32[32,4]{1,0:T(8,128)S(1)}, f32[32,4,1280]{2,1,0:T(4,128)S(1)}) fusion(pred[32,1280]{1,0:T(8,128)(4,1)S(1)} %broadcast_compare_fusion, f32[32,4,1280]{2,1,0:T(4,128)} %param.19, bf16[32,4,64]{2,1,0:T(4,128)(2,1)S(1)} %reshape.301, bf16[32,1280,1,128]{3,1,2,0:T(8,128)(2,1)} %param.18), kind=kOutput, calls=%fused_computation.16 | convolution fusion | flops 21626752 | bytes 11854336 | tf_op jit(solution)/shard_map/bkgd,blkd->bkgl/dot_general | solution.py:132
  43.2 1.7 %gather_fusion = f32[128]{0:T(128)S(1)} fusion(f32[32,4,1280]{2,1,0:T(4,128)S(1)} %copy-done.1, s32[128]{0:T(128)S(1)} %reshape.310), kind=kCustom, calls=%fused_computation | custom fusion | bytes 2560 | tf_op jit(solution)/shard_map/jit(take_along_axis)/gather | solution.py:144
  45.5 0.5 fusion.15
  46.4 7.2 %fusion.12 = f32[32,4,64]{2,1,0:T(4,128)S(1)} fusion(bf16[32,1280,1,128]{3,1,2,0:T(8,128)(2,1)} %param.18, f32[32,4,1280]{2,1,0:T(4,128)S(1)} %get-tuple-element.41, f32[32,4]{1,0:T(8,128)S(1)} %copy.157, pred[32,1280]{1,0:T(8,128)(4,1)S(1)} %broadcast_compare_fusion, f32[32,64]{1,0:T(8,128)S(1)} %get-tuple-element.33, f32[32,4]{1,0:T(8,128)S(1)} %copy.159), kind=kOutput, calls=%fused_computation.9 | convolution fusion | flops 21479424 | bytes 11224064 | tf_op jit(solution)/shard_map/bkgl,blkd->bkgd/dot_general | solution.py:164
  53.8 15.1 %all_to_all.10 = f32[16,134,64]{1,2,0:T(8,128)S(1)} all-to-all(f32[16,134,64]{1,2,0:T(8,128)S(1)} %broadcast_in_dim.98), channel_id=1, replica_groups=mesh['kv_0'=4,'kv_1'=4,'tp'=8] {'kv_0','kv_1'}, dimensions={0} | all-to-all | bytes 1097728 | tf_op jit(solution)/shard_map/all_to_all | solution.py:22
  68.9 0.3 fusion.54
  69.3 0.5 copy.181
  70.1 0.4 slice.161
  71.7 0.5 copy.166
  72.5 0.4 slice.136
  72.9 0.5 copy.177
  73.7 0.4 slice.152
  74.1 0.5 copy.187
  74.6 0.6 slice.133
  75.3 0.6 slice.137
  76.8 0.8 slice.138
  77.7 0.8 slice.141
  78.7 0.3 multiply_add_fusion.1
  79.1 0.7 slice.142
  79.8 0.7 slice.145
  80.8 0.6 bitcast_add_fusion
  82.2 0.4 fusion.22
  83.1 19.0 %all_to_all.11 = bf16[8,32,256]{2,1,0:T(8,128)(2,1)S(1)} all-to-all(bf16[8,32,256]{2,1,0:T(8,128)(2,1)S(1)} %broadcast_in_dim.99), channel_id=1, replica_groups=mesh['kv_0'=4,'kv_1'=4,'tp'=8] {'tp'}, dimensions={0} | all-to-all | bytes 262144 | tf_op jit(solution)/shard_map/all_to_all | solution.py:22
  102.1 0.6 reduce_sum.32
  (85 shorter events, 7.1 us)
Async XLA Ops:
  0.6 4.0 %copy-start = (bf16[4096,32]{0,1:T(8,128)(2,1)S(1)}, bf16[4096,32]{0,1:T(8,128)(2,1)}, u32[]{:S(2)}) copy-start(bf16[4096,32]{0,1:T(8,128)(2,1)} %param.16) | copy-start | bytes 786436
  0.6 42.2 %copy-start.3 = (s32[32]{0:T(128)S(1)}, s32[32]{0:T(128)}, u32[]{:S(2)}) copy-start(s32[32]{0:T(128)} %param.20) | copy-start | bytes 388
  0.7 42.5 %copy-start.1 = (f32[32,4,1280]{2,1,0:T(4,128)S(1)}, f32[32,4,1280]{2,1,0:T(4,128)}, u32[]{:S(2)}) copy-start(f32[32,4,1280]{2,1,0:T(4,128)} %param.19) | copy-start | bytes 1966084
  42.4 2.7 %copy-start.4 = (f32[4]{0:T(128)S(1)}, f32[4]{0:T(128)}, u32[]{:S(2)}) copy-start(f32[4]{0:T(128)} %param.17) | copy-start | bytes 52
  53.7 29.2 %copy-start.2 = (bf16[256,256]{1,0:T(8,128)(2,1)S(1)}, bf16[256,256]{1,0:T(8,128)(2,1)}, u32[]{:S(2)}) copy-start(bf16[256,256]{1,0:T(8,128)(2,1)} %param.21) | copy-start | bytes 393220
where the time goes:
time: 103 us
  blocking collectives  63 us (61%)
  matrix products  18.3 us (18%)
  local copies, waits for them, and re-layouts  14.7 us (14%)
  other arithmetic  5.54 us (5%)
  between operations  1.11 us (1%)
    all_to_all x2, blocking collectives, sent_to_all(): return lax.all_to_all(copies, axis, split_axis=0, concat_axis=0, tiled=True)  34 us
    psum x2, blocking collectives, by_axis(): array = lax.psum(array, axis)  29 us
    slice x16, local copies, waits for them, and re-layouts, combined_pairwise(): part[side::2]  7.47 us
    dot_general x1, matrix products, shards(): jnp.einsum('bkgl,blkd->bkgd', weights.astype(jnp.bfloat16), cached_vals,...  7.19 us
    dot_general x1, matrix products, shards(): jnp.einsum('bkgd,blkd->bkgl', query_head_rows, cached_keys, preferred_ele...  6.99 us

commit v1 on v0

v1 whole, which is shorter than its diff:
```python
import functools
import itertools

import jax
import jax.numpy as jnp
from jax import lax
from jax.experimental import pallas as pl
from jax.experimental.pallas import tpu as pltpu
from jax.sharding import Mesh
from jax.sharding import PartitionSpec as P

KV = ("kv_0", "kv_1")
ORDERS = (("kv_1", "kv_0"), ("kv_0", "kv_1"))
MESH = pl.DeviceIdType.MESH
NT = (((1,), (1,)), ((), ()))
norm_eps = 1e-05
masked_floor = -1e30
empty_peak = -1e29
f32, bf16 = jnp.float32, jnp.bfloat16


def iota(shape, axis):
    return lax.broadcasted_iota(jnp.int32, shape, axis)


def kernel(
    n_kv0,
    n_kv1,
    n_tp,
    tokens,
    gain,
    w_query,
    w_key,
    w_value,
    gate_rows,
    gate_bias,
    cache,
    cum,
    lengths,
    w_out,
    mixed,
    log_weight,
    tok_v,
    gain_v,
    wq_v,
    wkv_v,
    wg_v,
    wo_v,
    cache_v,
    cum_v,
    keys_t,
    cum_neg,
    biased,
    weights,
    qg_1,
    qg_2,
    new_1,
    new_2,
    val_1,
    val_2,
    stat_1,
    stat_2,
    out_x,
    load_sem,
    send_sem,
    recv_sem,
):
    place = {"kv_0": lax.axis_index("kv_0"), "kv_1": lax.axis_index("kv_1"), "tp": lax.axis_index("tp")}
    sizes = {"kv_0": n_kv0, "kv_1": n_kv1, "tp": n_tp}
    kv_index = place["kv_0"] * n_kv1 + place["kv_1"]
    batch, span = cache.shape[0], cache.shape[1]
    cols = tokens.shape[1]
    heads = cum.shape[1]
    head = cache.shape[2] // 2
    rows = heads * batch
    half = batch // 2
    width = cols * n_kv0 * n_kv1

    count = itertools.count()

    def load(src, dst):
        copy = pltpu.make_async_copy(src, dst, load_sem.at[next(count)])
        copy.start()
        return copy

    small = [
        load(tokens, tok_v),
        load(gain, gain_v),
        load(w_query, wq_v),
        load(w_key, wkv_v.at[pl.ds(0, head)]),
        load(w_value, wkv_v.at[pl.ds(head, head)]),
        load(gate_rows.at[:, pl.ds(pl.multiple_of(kv_index * cols, cols), cols)], wg_v.at[pl.ds(0, gate_rows.shape[0])]),
    ]
    cum_load = load(cum, cum_v)
    block = batch // 8
    cache_loads = [load(cache.at[pl.ds(k * block, block)], cache_v.at[pl.ds(k * block, block)]) for k in range(8)]
    wo_load = load(w_out, wo_v)

    barrier = pltpu.get_barrier_semaphore()
    for axis, size in sizes.items():
        for step in range(1, size):
            pl.semaphore_signal(
                barrier, inc=1, device_id={axis: lax.rem(place[axis] + step, size)}, device_id_type=MESH
            )

    numbers = itertools.count()
    sent = []

    def exchange(buffer, axis):
        size = sizes[axis]
        me = place[axis]
        waits = []
        for step in sorted(range(1, size), key=lambda s: -min(s, size - s)):
            number = next(numbers)
            source = lax.rem(me + size - step, size)
            out = pltpu.make_async_remote_copy(
                src_ref=buffer.at[me],
                dst_ref=buffer.at[me],
                send_sem=send_sem.at[number],
                recv_sem=recv_sem.at[number],
                device_id={axis: lax.rem(me + step, size)},
                device_id_type=MESH,
            )
            out.start()
            sent.append(out)
            waits.append(
                pltpu.make_async_remote_copy(
                    src_ref=buffer.at[source],
                    dst_ref=buffer.at[source],
                    send_sem=send_sem.at[number],
                    recv_sem=recv_sem.at[number],
                    device_id={axis: source},
                    device_id_type=MESH,
                )
            )
        return waits

    def arrived(waits):
        for wait in waits:
            wait.wait_recv()

    def total(buffer, size):
        acc = buffer[0].astype(f32)
        for k in range(1, size):
            acc = acc + buffer[k].astype(f32)
        return acc

    wg_v[gate_rows.shape[0] :, :] = jnp.zeros((wg_v.shape[0] - gate_rows.shape[0], cols), bf16)
    for copy in small:
        copy.wait()
    tokens_f = tok_v[...].astype(f32)
    squares = jnp.sum(tokens_f * tokens_f, axis=1, keepdims=True)
    normed = (tokens_f * gain_v[...]).astype(bf16)
    part_query = jnp.dot(normed, wq_v[...], preferred_element_type=f32).astype(bf16)
    part_gate = lax.dot_general(normed, wg_v[...], NT, preferred_element_type=f32)
    n_gates = gate_rows.shape[0]
    lane = iota((batch, 128), 1)
    part_gate = jnp.where(lane < n_gates, part_gate, squares).astype(bf16)
    part_new = lax.dot_general(normed, wkv_v[...], NT, preferred_element_type=f32).astype(bf16)
    for part in range(2):
        me = place[ORDERS[part][0]]
        chunk = slice(part * half, (part + 1) * half)
        qg_1[part, me, :, : heads * head] = part_query[chunk]
        qg_1[part, me, :, heads * head :] = part_gate[chunk]
        new_1[part, me] = part_new[chunk]

    pl.semaphore_wait(barrier, sum(size - 1 for size in sizes.values()))
    qg_waits = [exchange(qg_1.at[part], ORDERS[part][0]) for part in range(2)]
    new_waits = [exchange(new_1.at[part], ORDERS[part][0]) for part in range(2)]

    cum_load.wait()
    first_pos = kv_index * span
    length_rows = jnp.zeros((batch, 128), jnp.int32)
    for b in range(batch):
        length_rows = jnp.where(iota((batch, 128), 0) == b, lengths[b], length_rows)
    length_col = length_rows[:, :1] - first_pos
    last_parts = []
    for h in range(heads):
        last = jnp.zeros((batch, 128), f32)
        for n in range(span // 128):
            position = iota((batch, 128), 1) + n * 128
            value = cum_v[:, h, n * 128 : (n + 1) * 128]
            cum_neg[h * batch : (h + 1) * batch, n * 128 : (n + 1) * 128] = jnp.where(
                position < length_col, -value, masked_floor
            )
            last = last + jnp.where(position == length_col - 1, value, 0.0)
        last_parts.append(jnp.sum(last, axis=1, keepdims=True))
    last_cum = jnp.concatenate(last_parts, axis=0)
    holds = (length_col > 0) & (length_col <= span)
    holds = jnp.concatenate([jnp.where(holds, 1, 0)] * heads, axis=0) > 0

    def transpose_keys(first, count):
        def one(b, carry):
            flipped = cache_v[b].T
            keys_t[pl.ds(pl.multiple_of(b * head, head), head), :] = flipped[:head]
            return carry

        lax.fori_loop(first, first + count, one, 0)

    for part in range(2):
        arrived(qg_waits[part])
        me = place[ORDERS[part][1]]
        qg_2[part, me] = total(qg_1.at[part], sizes[ORDERS[part][0]]).astype(bf16)
    qg_waits = [exchange(qg_2.at[part], ORDERS[part][1]) for part in range(2)]
    for part in range(2):
        arrived(new_waits[part])
        me = place[ORDERS[part][1]]
        new_2[part, me] = total(new_1.at[part], sizes[ORDERS[part][0]]).astype(bf16)
    new_waits = [exchange(new_2.at[part], ORDERS[part][1]) for part in range(2)]

    for copy in cache_loads:
        copy.wait()
    transpose_keys(0, batch)

    for part in range(2):
        arrived(qg_waits[part])
    sums = jnp.concatenate([total(qg_2.at[part], sizes[ORDERS[part][1]]) for part in range(2)], axis=0)
    gates = sums[:, heads * head :]
    row_scale = lax.rsqrt(gates[:, n_gates : n_gates + 1] / width + norm_eps)
    query = (row_scale * sums[:, : heads * head]).astype(bf16).astype(f32)
    first_gate = place["tp"] * heads
    log_gate = []
    for h in range(heads):
        logit = jnp.sum(jnp.where(lane == first_gate + h, gates, 0.0), axis=1, keepdims=True)
        logit = row_scale * logit + gate_bias[h]
        log_gate.append(jnp.minimum(logit, 0.0) - jnp.log1p(jnp.exp(-jnp.abs(logit))))
    cum_query = last_cum + jnp.concatenate(log_gate, axis=0)

    doubled = []
    for pair in range(heads // 2):
        two = query[:, pair * 128 : (pair + 1) * 128]
        turned = pltpu.roll(two, 64, 1)
        doubled.append(jnp.where(lane < head, two, turned))
        doubled.append(jnp.where(lane < head, turned, two))
    doubled = jnp.concatenate(doubled, axis=0)
    row_of = iota((rows, 128), 0) % batch
    lane_of = iota((rows, 128), 1)
    side = jnp.where(lane_of < head, 0, 1)
    inv_root = head ** (-0.5)
    scaled = doubled * inv_root
    spread = jnp.concatenate(
        [jnp.where(row_of == 2 * p + side, scaled, 0.0).astype(bf16) for p in range(batch // 2)], axis=1
    )

    tile = 256
    peak = jnp.full((rows, 128), masked_floor, f32)
    for n in range(span // tile):
        cut = slice(n * tile, (n + 1) * tile)
        score = jnp.dot(spread, keys_t[:, cut], preferred_element_type=f32) + cum_neg[:, cut]
        biased[:, cut] = score
        for k in range(tile // 128):
            peak = jnp.maximum(peak, score[:, k * 128 : (k + 1) * 128])

    for part in range(2):
        arrived(new_waits[part])
    new_rows = jnp.concatenate([total(new_2.at[part], sizes[ORDERS[part][1]]) for part in range(2)], axis=0)
    new_rows = (row_scale * new_rows).astype(bf16).astype(f32)
    new_rows = jnp.concatenate([new_rows] * heads, axis=0)
    new_biased = (
        jnp.sum(jnp.where(lane_of < head, doubled * new_rows, 0.0), axis=1, keepdims=True) * inv_root
        - cum_query
    )

    peak = jnp.max(peak, axis=1, keepdims=True)
    peak = jnp.where(holds, jnp.maximum(peak, new_biased), peak)
    peak = jnp.maximum(peak, empty_peak)
    sums = jnp.zeros((rows, 128), f32)
    for n in range(span // 128):
        cut = slice(n * 128, (n + 1) * 128)
        weight = jnp.exp(biased[:, cut] - peak)
        sums = sums + weight
        weights[:, cut] = weight.astype(bf16)
    new_weight = jnp.where(holds, jnp.exp(new_biased - peak), 0.0)
    weight_sum = jnp.sum(sums, axis=1, keepdims=True) + new_weight

    values = new_weight.astype(bf16).astype(f32) * new_rows
    for p in range(batch // 2):
        both = jnp.concatenate([cache_v[2 * p], cache_v[2 * p + 1]], axis=1)
        out = jnp.dot(weights[...], both, preferred_element_type=f32)
        values = (
            values
            + jnp.where(row_of == 2 * p, out[:, :128], 0.0)
            + jnp.where(row_of == 2 * p + 1, out[:, 128:], 0.0)
        )

    diagonal = iota((rows, 128), 0) == lane_of

    def as_row(column):
        return jnp.sum(jnp.where(diagonal, column, 0.0), axis=0, keepdims=True)

    sub = iota((8, 128), 0)
    anchor = jnp.where(holds, cum_query, 0.0)
    stats = jnp.where(sub == 0, as_row(peak), jnp.where(sub == 1, as_row(weight_sum), as_row(anchor)))
    for part in range(2):
        me = place[ORDERS[part][0]]
        low = values[2 * part * batch : (2 * part + 1) * batch]
        high = values[(2 * part + 1) * batch : (2 * part + 2) * batch]
        val_1[part, me] = jnp.where(lane < head, pltpu.roll(low, 64, 1), high).astype(bf16)
        stat_1[part, me] = stats
    stat_waits = [exchange(stat_1.at[part], ORDERS[part][0]) for part in range(2)]
    val_waits = [exchange(val_1.at[part], ORDERS[part][0]) for part in range(2)]

    def combined(part, vals, stat, size, final):
        found = [stat[k] for k in range(size)]
        peak = functools.reduce(jnp.maximum, [s[0:1] for s in found])
        factors = [jnp.exp(s[0:1] - peak) for s in found]
        weight_sum = sum(s[1:2] * f for s, f in zip(found, factors))
        anchor = sum(s[2:3] for s in found)
        if final:
            factors = [f / weight_sum for f in factors]
        table = jnp.zeros((8, 128), f32)
        for k, f in enumerate(factors):
            table = jnp.where(sub == k, f, table)
        columns = table.T
        acc = None
        for k in range(size):
            low = columns[2 * part * batch : (2 * part + 1) * batch, k : k + 1]
            high = columns[(2 * part + 1) * batch : (2 * part + 2) * batch, k : k + 1]
            term = vals[k].astype(f32) * jnp.where(lane < head, low, high)
            acc = term if acc is None else acc + term
        return peak, weight_sum, anchor, acc

    for part in range(2):
        arrived(stat_waits[part])
        arrived(val_waits[part])
        first, second = ORDERS[part]
        peak, weight_sum, anchor, acc = combined(part, val_1.at[part], stat_1.at[part], sizes[first], False)
        me = place[second]
        val_2[part, me] = acc.astype(bf16)
        stat_2[part, me] = jnp.where(sub == 0, peak, jnp.where(sub == 1, weight_sum, anchor))
    stat_waits = [exchange(stat_2.at[part], ORDERS[part][1]) for part in range(2)]
    val_waits = [exchange(val_2.at[part], ORDERS[part][1]) for part in range(2)]

    wo_load.wait()
    attended, logs = [], []
    for part in range(2):
        arrived(stat_waits[part])
        arrived(val_waits[part])
        peak, weight_sum, anchor, acc = combined(
            part, val_2.at[part], stat_2.at[part], sizes[ORDERS[part][1]], True
        )
        attended.append(acc)
        logs.append(peak + jnp.log(weight_sum) + anchor)
    attended = jnp.concatenate(attended, axis=1).astype(bf16)
    part_out = jnp.dot(attended, wo_v[...], preferred_element_type=f32)
    out_x[place["tp"]] = part_out.astype(bf16)
    out_waits = exchange(out_x, "tp")

    logs = jnp.where(iota((8, 128), 1) < rows // 2, logs[0], logs[1]).T
    found = jnp.zeros((batch, heads), f32)
    for h in range(heads):
        found = jnp.where(iota((batch, heads), 1) == h, logs[h * batch : (h + 1) * batch, :1], found)
    log_weight[...] = found

    arrived(out_waits)
    mixed[...] = total(out_x, n_tp).astype(bf16)
    for out in sent:
        out.wait_send()


def shards(*args):
    (tokens, gain, w_query, w_key, w_value, gate_w, gate_bias, cache, cum, lengths, w_out) = args
    n_kv0, n_kv1, n_tp = (lax.axis_size(a) for a in ("kv_0", "kv_1", "tp"))
    batch, cols = tokens.shape
    span, head = cache.shape[1], cache.shape[3] // 2
    heads = cum.shape[1]
    rows = heads * batch
    half = batch // 2
    copies = 2 * (4 * 2 * (n_kv0 + n_kv1 - 2) // 2) + n_tp - 1
    anywhere = pl.BlockSpec(memory_space=pl.ANY)
    scalars = pl.BlockSpec(memory_space=pltpu.SMEM)
    n = max(n_kv0, n_kv1)
    in_specs = [anywhere] * 6 + [scalars] + [anywhere] * 2 + [scalars, anywhere]
    return pl.pallas_call(
        functools.partial(kernel, n_kv0, n_kv1, n_tp),
        out_shape=(
            jax.ShapeDtypeStruct((batch, w_out.shape[1]), bf16),
            jax.ShapeDtypeStruct((batch, heads), f32),
        ),
        in_specs=in_specs,
        out_specs=(pl.BlockSpec(memory_space=pltpu.VMEM), pl.BlockSpec(memory_space=pltpu.VMEM)),
        scratch_shapes=[
            pltpu.VMEM((batch, cols), bf16),
            pltpu.VMEM((1, cols), f32),
            pltpu.VMEM(w_query.shape, bf16),
            pltpu.VMEM((2 * head, cols), bf16),
            pltpu.VMEM((128, cols), bf16),
            pltpu.VMEM(w_out.shape, bf16),
            pltpu.VMEM((batch, span, 2 * head), bf16),
            pltpu.VMEM(cum.shape, f32),
            pltpu.VMEM((batch * head, span), bf16),
            pltpu.VMEM((rows, span), f32),
            pltpu.VMEM((rows, span), f32),
            pltpu.VMEM((rows, span), bf16),
            pltpu.VMEM((2, n, half, heads * head + 128), bf16),
            pltpu.VMEM((2, n, half, heads * head + 128), bf16),
            pltpu.VMEM((2, n, half, 128), bf16),
            pltpu.VMEM((2, n, half, 128), bf16),
            pltpu.VMEM((2, n, batch, 128), bf16),
            pltpu.VMEM((2, n, batch, 128), bf16),
            pltpu.VMEM((2, n, 8, 128), f32),
            pltpu.VMEM((2, n, 8, 128), f32),
            pltpu.VMEM((n_tp, batch, w_out.shape[1]), bf16),
            pltpu.SemaphoreType.DMA((16,)),
            pltpu.SemaphoreType.DMA((64,)),
            pltpu.SemaphoreType.DMA((64,)),
        ],
        compiler_params=pltpu.CompilerParams(
            collective_id=0, has_side_effects=True, vmem_limit_bytes=60 * 1024 * 1024
        ),
    )(
        tokens,
        gain.reshape(1, cols),
        w_query,
        w_key.T,
        w_value.T,
        gate_w.T,
        gate_bias,
        cache.reshape(batch, span, 2 * head),
        cum,
        lengths,
        w_out,
    )


def solution(mesh):
    torus = Mesh(mesh.devices.reshape(4, 4, mesh.shape["tp"]), ("kv_0", "kv_1", "tp"))
    placed = (
        P(None, KV),
        P(KV),
        P(KV, "tp"),
        P(KV, "tp"),
        P(KV, "tp"),
        P(),
        P("tp"),
        P(None, KV, "tp", None),
        P(None, "tp", KV),
        P(),
        P("tp", KV),
    )
    return jax.shard_map(
        shards, mesh=torus, in_specs=placed, out_specs=(P(None, KV), P(None, "tp")), check_vma=False
    )
```

time: 103 us -> 36.9 us (0.36)
  blocking collectives: 63 us -> 0 us
  Pallas kernels: 0 us -> 33.2 us
  matrix products: 18.3 us -> 0 us
  local copies, waits for them, and re-layouts: 14.7 us -> 2.69 us
  other arithmetic: 5.54 us -> 0 us
    all_to_all x2 -> x0, blocking collectives: 34 us -> none  [sent_to_all(): return lax.all_to_all(copies, axis, split_axis=0, concat_axis=0, tiled=True)]
    pallas_call x0 -> x1, Pallas kernels: none -> 33.2 us  [shards(): pl.pallas_call(functools.partial(kernel, n_kv0, n_kv1, n_tp), out_shape=(...]
    psum x2 -> x0, blocking collectives: 29 us -> none  [by_axis(): array = lax.psum(array, axis)]
    dot_general x8 -> x0, matrix products: 18.3 us -> none  [the longest x1 7.19 us: shards(): jnp.einsum('bkgl,blkd->bkgd', weights.astype(jnp.bfloat16), cached_vals,...]
    slice x21 -> x0, local copies, waits for them, and re-layouts: 9.36 us -> none  [the longest x16 7.47 us: combined_pairwise(): part[side::2]]
    add x15 -> x0, other arithmetic: 2.23 us -> none  [the longest x4 1.39 us: combine_parts(): vals_one * factor_one[..., None] + vals_two * factor_two[..., None]]
    gather x5 -> x0, local copies, waits for them, and re-layouts: 2.05 us -> none  [shards(): jnp.take_along_axis(cum_gates, jnp.broadcast_to(last_index[:, None, None]...]
    reduce_sum x3 -> x0, other arithmetic: 2.02 us -> none  [the longest x1 0.9 us: shards(): squares = jnp.sum(tokens_f * tokens_f, axis=1)]
where the time goes in v1:
time: 36.9 us; the launch traced here: 36.6 us
  Pallas kernels  33.2 us (90%)
  local copies, waits for them, and re-layouts  2.69 us (7%)
  between operations  0.64 us (2%)
    pallas_call x1, Pallas kernels, shards(): pl.pallas_call(functools.partial(kernel, n_kv0, n_kv1, n_tp), out_shape=(...  33.2 us
    pallas_call x1, local copies, waits for them, and re-layouts, shards(): pl.pallas_call(functools.partial(kernel, n_kv0, n_kv1, n_tp), out_shape=(...  1.37 us
    unnamed x1, local copies, waits for them, and re-layouts  1.32 us

profile of v1, /device:TPU:1, one launch (start us, length us, event | category | flops | bytes accessed | tf_op | source)
XLA Modules:
  0.0 36.6 jit_solution(3182625852120554377)
XLA Ops:
  0.6 33.2 %shard_map.122 = (bf16[32,256]{1,0:T(8,128)(2,1)}, f32[32,4]{1,0:T(8,128)}) custom-call(bf16[32,256]{1,0:T(8,128)(2,1)} %tokens.1, f32[1,256]{1,0:T(1,128)} %bitcast.9, bf16[256,256]{1,0:T(8,128)(2,1)} %w_query.1, bf16[64,256]{1,0:T(8,128)(2,1)} %bitcast.7, bf16[64,256]{1,0:T(8,128)(2,1)} %bitcast.8, bf16[32,4096]{1,0:T(8,128)(2,1)} %bitcast.6, f32[4]{0:T(128)} %gate_bias.1, ...), custom_call_target="tpu_custom_call" | custom-call | tf_op jit(solution)/shard_map/pallas_call | solution.py:374
  33.9 1.4 %copy.13 = f32[32,4]{0,1:T(4,128)} copy(f32[32,4]{1,0:T(8,128)} %get-tuple-element.3) | data formatting | bytes 1024 | tf_op jit(solution)/shard_map/pallas_call | solution.py:374
  35.2 1.3 %copy.15 = bf16[32,256]{1,0:T(8,128)(2,1)} copy(bf16[32,256]{1,0:T(8,128)(2,1)} %get-tuple-element.6) | data formatting | bytes 32768

commit v2 on v1

v2 whole, which is shorter than its diff:
```python
import functools
import itertools

import jax
import jax.numpy as jnp
from jax import lax
from jax.experimental import pallas as pl
from jax.experimental.pallas import tpu as pltpu
from jax.sharding import Mesh
from jax.sharding import PartitionSpec as P

KV = ("kv_0", "kv_1")
MESH = pl.DeviceIdType.MESH
NT = (((1,), (1,)), ((), ()))
norm_eps = 1e-05
masked_floor = -1e30
empty_peak = -1e29
f32, bf16 = jnp.float32, jnp.bfloat16


def iota(shape, axis):
    return lax.broadcasted_iota(jnp.int32, shape, axis)


def hops(offset, sizes):
    return sum(min(o, n - o) for o, n in zip(offset, sizes))


def kernel(
    n_kv0,
    n_kv1,
    n_tp,
    tokens,
    gain,
    w_query,
    w_key,
    w_value,
    gate_rows,
    gate_bias,
    cache,
    cum,
    lengths,
    w_out,
    mixed,
    log_weight,
    tok_v,
    gain_v,
    wq_v,
    wkv_v,
    wg_v,
    wo_v,
    bias_s,
    len_s,
    cache_v,
    cum_v,
    keys_t,
    cum_neg,
    biased,
    weights,
    query_x,
    gate_x,
    new_x,
    val_x,
    stat_x,
    out_x,
    load_sem,
    send_sem,
    recv_sem,
):
    at = tuple(lax.axis_index(a) for a in ("kv_0", "kv_1", "tp"))
    sizes = (n_kv0, n_kv1, n_tp)
    n_kv = n_kv0 * n_kv1
    kv_index = at[0] * n_kv1 + at[1]
    batch, span = cache.shape[0], cache.shape[1]
    cols = tokens.shape[1]
    heads = cum.shape[1]
    head = cache.shape[2] // 2
    rows = heads * batch
    half = batch // 2
    width = cols * n_kv
    n_gates = gate_rows.shape[0]

    count = itertools.count()

    def load(src, dst):
        copy = pltpu.make_async_copy(src, dst, load_sem.at[next(count)])
        copy.start()
        return copy

    mine = gate_rows.at[:, pl.ds(pl.multiple_of(kv_index * cols, cols), cols)]
    small = [
        load(tokens, tok_v),
        load(gain, gain_v),
        load(w_query, wq_v),
        load(mine, wg_v.at[pl.ds(0, n_gates)]),
        load(mine, wg_v.at[pl.ds(64, n_gates)]),
        load(w_key, wkv_v.at[pl.ds(0, head)]),
        load(w_value, wkv_v.at[pl.ds(head, head)]),
    ]

    kv_offsets = [(a, b, 0) for a in range(n_kv0) for b in range(n_kv1) if a or b]
    tp_offsets = [(0, 0, c) for c in range(1, n_tp)]
    kv_offsets.sort(key=lambda o: -hops(o, sizes))
    tp_offsets.sort(key=lambda o: -hops(o, sizes))

    def peer(offset, sign=1):
        return tuple(
            lax.rem(p + (o if sign > 0 else n - o), n) if o else p for p, o, n in zip(at, offset, sizes)
        )

    barrier = pltpu.get_barrier_semaphore()
    for offset in kv_offsets + tp_offsets:
        pl.semaphore_signal(barrier, inc=1, device_id=peer(offset), device_id_type=MESH)

    scalar_loads = [load(lengths, len_s), load(gate_bias, bias_s)]
    cum_load = load(cum, cum_v)
    block = batch // 8
    first_cache = next(count)
    for k in range(8):
        pltpu.make_async_copy(
            cache.at[pl.ds(k * block, block)],
            cache_v.at[pl.ds(k * block, block)],
            load_sem.at[first_cache + k],
        ).start()
    for k in range(7):
        next(count)
    wo_load = load(w_out, wo_v)

    numbers = itertools.count()
    sent = []

    def slot(place, offsets):
        return place[0] * n_kv1 + place[1] if offsets is kv_offsets else place[2]

    def exchange(buffer, offsets):
        waits = []
        for offset in offsets:
            number = next(numbers)
            there, source = peer(offset), peer(offset, -1)
            me, came = slot(at, offsets), slot(source, offsets)
            out = pltpu.make_async_remote_copy(
                src_ref=buffer.at[me],
                dst_ref=buffer.at[me],
                send_sem=send_sem.at[number],
                recv_sem=recv_sem.at[number],
                device_id=there,
                device_id_type=MESH,
            )
            out.start()
            sent.append(out)
            waits.append(
                (
                    came,
                    pltpu.make_async_remote_copy(
                        src_ref=buffer.at[came],
                        dst_ref=buffer.at[came],
                        send_sem=send_sem.at[number],
                        recv_sem=recv_sem.at[number],
                        device_id=source,
                        device_id_type=MESH,
                    ),
                )
            )
        return waits[::-1]

    wg_v[n_gates:64, :] = jnp.zeros((64 - n_gates, cols), bf16)
    wg_v[64 + n_gates :, :] = jnp.zeros((64 - n_gates, cols), bf16)
    for copy in small[:5]:
        copy.wait()
    tokens_f = tok_v[...].astype(f32)
    squares = jnp.sum(tokens_f * tokens_f, axis=1, keepdims=True)
    normed = (tokens_f * gain_v[...]).astype(bf16)
    lane = iota((batch, 128), 1)
    half_lane = iota((half, 128), 1)
    query_x[kv_index] = jnp.dot(normed, wq_v[...], preferred_element_type=f32).astype(bf16)
    part_gate = lax.dot_general(normed, wg_v[...], NT, preferred_element_type=f32)
    part_gate = jnp.where(lane % 64 < n_gates, part_gate, squares)
    gate_x[kv_index] = jnp.where(half_lane < 64, part_gate[:half], part_gate[half:]).astype(bf16)

    pl.semaphore_wait(barrier, len(kv_offsets) + len(tp_offsets))
    query_waits = exchange(query_x, kv_offsets)
    gate_waits = exchange(gate_x, kv_offsets)
    for copy in small[5:]:
        copy.wait()
    new_x[kv_index] = lax.dot_general(normed, wkv_v[...], NT, preferred_element_type=f32).astype(bf16)
    new_waits = exchange(new_x, kv_offsets)

    for copy in scalar_loads:
        copy.wait()
    cum_load.wait()
    first_pos = kv_index * span
    length_rows = jnp.zeros((batch, 128), jnp.int32)
    for b in range(batch):
        length_rows = jnp.where(iota((batch, 128), 0) == b, len_s[b], length_rows)
    length_col = length_rows[:, :1] - first_pos
    last_parts = []
    for h in range(heads):
        last = jnp.zeros((batch, 128), f32)
        for n in range(span // 128):
            position = iota((batch, 128), 1) + n * 128
            value = cum_v[:, h, n * 128 : (n + 1) * 128]
            cum_neg[h * batch : (h + 1) * batch, n * 128 : (n + 1) * 128] = jnp.where(
                position < length_col, -value, masked_floor
            )
            last = last + jnp.where(position == length_col - 1, value, 0.0)
        last_parts.append(jnp.sum(last, axis=1, keepdims=True))
    last_cum = jnp.concatenate(last_parts, axis=0)
    holds = (length_col > 0) & (length_col <= span)
    holds = jnp.concatenate([jnp.where(holds, 1, 0)] * heads, axis=0) > 0

    def flip(k, carry):
        pltpu.make_async_copy(
            cache.at[pl.ds(k * block, block)],
            cache_v.at[pl.ds(k * block, block)],
            load_sem.at[first_cache + k],
        ).wait()
        for j in range(block):
            b = k * block + j
            keys_t[pl.ds(pl.multiple_of(b * head, head), head), :] = cache_v[b].T[:head]
        return carry

    lax.fori_loop(0, 8, flip, 0)

    sum_query = query_x[kv_index].astype(f32)
    for came, wait in query_waits:
        wait.wait_recv()
        sum_query = sum_query + query_x[came].astype(f32)
    gates = gate_x[kv_index].astype(f32)
    for came, wait in gate_waits:
        wait.wait_recv()
        gates = gates + gate_x[came].astype(f32)
    total_squares = jnp.concatenate(
        [gates[:, n_gates : n_gates + 1], gates[:, 64 + n_gates : 65 + n_gates]], axis=0
    )
    row_scale = lax.rsqrt(total_squares / width + norm_eps)
    query = (row_scale * sum_query).astype(bf16).astype(f32)
    log_gate = []
    for h in range(heads):
        pick = at[2] * heads + h
        logit = jnp.concatenate(
            [
                jnp.sum(jnp.where(half_lane == pick + 64 * part, gates, 0.0), axis=1, keepdims=True)
                for part in range(2)
            ],
            axis=0,
        )
        logit = row_scale * logit + bias_s[h]
        log_gate.append(jnp.minimum(logit, 0.0) - jnp.log1p(jnp.exp(-jnp.abs(logit))))
    cum_query = last_cum + jnp.concatenate(log_gate, axis=0)

    doubled = []
    for pair in range(heads // 2):
        two = query[:, pair * 128 : (pair + 1) * 128]
        turned = pltpu.roll(two, 64, 1)
        doubled.append(jnp.where(lane < head, two, turned))
        doubled.append(jnp.where(lane < head, turned, two))
    doubled = jnp.concatenate(doubled, axis=0)
    row_of = iota((rows, 128), 0) % batch
    lane_of = iota((rows, 128), 1)
    side = jnp.where(lane_of < head, 0, 1)
    inv_root = head ** (-0.5)
    scaled = doubled * inv_root
    spread = jnp.concatenate(
        [jnp.where(row_of == 2 * p + side, scaled, 0.0).astype(bf16) for p in range(batch // 2)], axis=1
    )

    tile = 256
    peak = jnp.full((rows, 128), masked_floor, f32)
    for n in range(span // tile):
        cut = slice(n * tile, (n + 1) * tile)
        score = jnp.dot(spread, keys_t[:, cut], preferred_element_type=f32) + cum_neg[:, cut]
        biased[:, cut] = score
        for k in range(tile // 128):
            peak = jnp.maximum(peak, score[:, k * 128 : (k + 1) * 128])

    new_rows = new_x[kv_index].astype(f32)
    for came, wait in new_waits:
        wait.wait_recv()
        new_rows = new_rows + new_x[came].astype(f32)
    new_rows = (row_scale * new_rows).astype(bf16).astype(f32)
    new_rows = jnp.concatenate([new_rows] * heads, axis=0)
    new_biased = (
        jnp.sum(jnp.where(lane_of < head, doubled * new_rows, 0.0), axis=1, keepdims=True) * inv_root
        - cum_query
    )

    peak = jnp.max(peak, axis=1, keepdims=True)
    peak = jnp.where(holds, jnp.maximum(peak, new_biased), peak)
    peak = jnp.maximum(peak, empty_peak)
    sums = jnp.zeros((rows, 128), f32)
    for n in range(span // 128):
        cut = slice(n * 128, (n + 1) * 128)
        weight = jnp.exp(biased[:, cut] - peak)
        sums = sums + weight
        weights[:, cut] = weight.astype(bf16)
    new_weight = jnp.where(holds, jnp.exp(new_biased - peak), 0.0)
    weight_sum = jnp.sum(sums, axis=1, keepdims=True) + new_weight

    diagonal = iota((rows, 128), 0) == lane_of

    def as_row(column):
        return jnp.sum(jnp.where(diagonal, column, 0.0), axis=0, keepdims=True)

    sub = iota((8, 128), 0)
    anchor = jnp.where(holds, cum_query, 0.0)
    stat_x[kv_index] = jnp.where(
        sub == 0, as_row(peak), jnp.where(sub == 1, as_row(weight_sum), as_row(anchor))
    )
    stat_waits = exchange(stat_x, kv_offsets)

    values = new_weight.astype(bf16).astype(f32) * new_rows
    for p in range(batch // 2):
        both = jnp.concatenate([cache_v[2 * p], cache_v[2 * p + 1]], axis=1)
        out = jnp.dot(weights[...], both, preferred_element_type=f32)
        values = (
            values
            + jnp.where(row_of == 2 * p, out[:, :128], 0.0)
            + jnp.where(row_of == 2 * p + 1, out[:, 128:], 0.0)
        )
    val_x[kv_index] = values.T[head:].astype(bf16)
    val_waits = exchange(val_x, kv_offsets)

    wo_load.wait()
    for _, wait in stat_waits:
        wait.wait_recv()
    peaks = stat_x[:, 0, :]
    peak = jnp.max(peaks, axis=0, keepdims=True)
    factors = jnp.exp(peaks - peak)
    weight_sum = jnp.sum(stat_x[:, 1, :] * factors, axis=0, keepdims=True)
    logs = peak + jnp.log(weight_sum) + jnp.sum(stat_x[:, 2, :], axis=0, keepdims=True)
    factors = factors / weight_sum
    log_weight[...] = jnp.concatenate([logs[:, h * batch : (h + 1) * batch] for h in range(heads)], axis=0)
    for _, wait in val_waits:
        wait.wait_recv()
    acc = val_x[0].astype(f32) * factors[0:1]
    for k in range(1, n_kv):
        acc = acc + val_x[k].astype(f32) * factors[k : k + 1]
    attended = acc.T.astype(bf16)
    part_out = jnp.zeros((batch, w_out.shape[1]), f32)
    for h in range(heads):
        part_out = part_out + jnp.dot(
            attended[h * batch : (h + 1) * batch],
            wo_v[h * head : (h + 1) * head],
            preferred_element_type=f32,
        )
    out_x[at[2]] = part_out.astype(bf16)
    out_waits = exchange(out_x, tp_offsets)
    for _, wait in out_waits:
        wait.wait_recv()
    acc = out_x[0].astype(f32)
    for k in range(1, n_tp):
        acc = acc + out_x[k].astype(f32)
    mixed[...] = acc.astype(bf16)
    for out in sent:
        out.wait_send()


def shards(*args):
    (tokens, gain, w_query, w_key, w_value, gate_w, gate_bias, cache, cum, lengths, w_out) = args
    n_kv0, n_kv1, n_tp = (lax.axis_size(a) for a in ("kv_0", "kv_1", "tp"))
    n_kv = n_kv0 * n_kv1
    batch, cols = tokens.shape
    span, head = cache.shape[1], cache.shape[3] // 2
    heads = cum.shape[1]
    rows = heads * batch
    half = batch // 2
    copies = 5 * (n_kv - 1) + n_tp - 1
    anywhere = pl.BlockSpec(memory_space=pl.ANY)
    near = pl.BlockSpec(memory_space=pltpu.VMEM)
    mixed, logs = pl.pallas_call(
        functools.partial(kernel, n_kv0, n_kv1, n_tp),
        out_shape=(
            pltpu.VMEM((batch, w_out.shape[1]), bf16),
            pltpu.VMEM((heads, batch), f32),
        ),
        in_specs=[anywhere] * len(args),
        out_specs=(near, near),
        scratch_shapes=[
            pltpu.VMEM((batch, cols), bf16),
            pltpu.VMEM((1, cols), f32),
            pltpu.VMEM(w_query.shape, bf16),
            pltpu.VMEM((2 * head, cols), bf16),
            pltpu.VMEM((128, cols), bf16),
            pltpu.VMEM(w_out.shape, bf16),
            pltpu.SMEM(gate_bias.shape, f32),
            pltpu.SMEM(lengths.shape, jnp.int32),
            pltpu.VMEM((batch, span, 2 * head), bf16),
            pltpu.VMEM(cum.shape, f32),
            pltpu.VMEM((batch * head, span), bf16),
            pltpu.VMEM((rows, span), f32),
            pltpu.VMEM((rows, span), f32),
            pltpu.VMEM((rows, span), bf16),
            pltpu.VMEM((n_kv, batch, heads * head), bf16),
            pltpu.VMEM((n_kv, half, 128), bf16),
            pltpu.VMEM((n_kv, batch, 2 * head), bf16),
            pltpu.VMEM((n_kv, head, rows), bf16),
            pltpu.VMEM((n_kv, 8, rows), f32),
            pltpu.VMEM((n_tp, batch, w_out.shape[1]), bf16),
            pltpu.SemaphoreType.DMA((24,)),
            pltpu.SemaphoreType.DMA((copies,)),
            pltpu.SemaphoreType.DMA((copies,)),
        ],
        compiler_params=pltpu.CompilerParams(
            collective_id=0, has_side_effects=True, vmem_limit_bytes=60 * 1024 * 1024
        ),
    )(
        tokens,
        gain.reshape(1, cols),
        w_query,
        w_key.T,
        w_value.T,
        gate_w.T,
        gate_bias,
        cache.reshape(batch, span, 2 * head),
        cum,
        lengths,
        w_out,
    )
    return mixed, logs.T


def solution(mesh):
    torus = Mesh(mesh.devices.reshape(4, 4, mesh.shape["tp"]), ("kv_0", "kv_1", "tp"))
    placed = (
        P(None, KV),
        P(KV),
        P(KV, "tp"),
        P(KV, "tp"),
        P(KV, "tp"),
        P(),
        P("tp"),
        P(None, KV, "tp", None),
        P(None, "tp", KV),
        P(),
        P("tp", KV),
    )
    return jax.shard_map(
        shards, mesh=torus, in_specs=placed, out_specs=(P(None, KV), P(None, "tp")), check_vma=False
    )
```

time: 36.9 us -> 32.4 us (0.88)
  Pallas kernels: 33.2 us -> 30.4 us
  local copies, waits for them, and re-layouts: 2.69 us -> 1.19 us
    pallas_call x1, Pallas kernels: 33.2 us -> 30.4 us  [shards(): pl.pallas_call(functools.partial(kernel, n_kv0, n_kv1, n_tp), out_shape=(...]
    pallas_call x1 -> x0, local copies, waits for them, and re-layouts: 1.37 us -> none  [shards(): pl.pallas_call(functools.partial(kernel, n_kv0, n_kv1, n_tp), out_shape=(...]
    unnamed x1 -> x2, local copies, waits for them, and re-layouts: 1.32 us -> 1.19 us
where the time goes in v2:
time: 32.4 us; the launch traced here: 32.3 us
  Pallas kernels  30.4 us (94%)
  local copies, waits for them, and re-layouts  1.19 us (4%)
  between operations  0.64 us (2%)
    pallas_call x1, Pallas kernels, shards(): pl.pallas_call(functools.partial(kernel, n_kv0, n_kv1, n_tp), out_shape=(...  30.4 us
    unnamed x2, local copies, waits for them, and re-layouts  1.19 us

profile of v2, /device:TPU:1, one launch (start us, length us, event | category | flops | bytes accessed | tf_op | source)
XLA Modules:
  0.0 32.3 jit_solution(16726168962954713835)
XLA Ops:
  0.6 30.4 %shard_map.122 = (bf16[32,256]{1,0:T(8,128)(2,1)S(1)}, f32[4,32]{1,0:T(4,128)S(1)}) custom-call(bf16[32,256]{1,0:T(8,128)(2,1)} %tokens.1, f32[1,256]{1,0:T(1,128)} %bitcast.11, bf16[256,256]{1,0:T(8,128)(2,1)} %w_query.1, bf16[64,256]{1,0:T(8,128)(2,1)} %bitcast.9, bf16[64,256]{1,0:T(8,128)(2,1)} %bitcast.10, bf16[32,4096]{1,0:T(8,128)(2,1)} %bitcast.8, ...), custom_call_target="tpu_custom_call" | custom-call | tf_op jit(solution)/shard_map/pallas_call | solution.py:370
  31.1 0.6 %copy.15 = bf16[32,256]{1,0:T(8,128)(2,1)} copy(bf16[32,256]{1,0:T(8,128)(2,1)S(1)} %get-tuple-element.6) | data formatting | bytes 32768
  31.7 0.6 %copy.16 = f32[32,4]{0,1:T(4,128)} copy(f32[32,4]{0,1:T(4,128)S(1)} %bitcast.6) | data formatting | bytes 1024

commit v3 on v2

--- a/solution.py
+++ b/solution.py
@@ -54,11 +54,11 @@
     cache_v,
     cum_v,
     keys_t,
+    packed,
     cum_neg,
     biased,
     weights,
     query_x,
-    gate_x,
     new_x,
     val_x,
     stat_x,
@@ -76,114 +76,98 @@
     heads = cum.shape[1]
     head = cache.shape[2] // 2
     rows = heads * batch
-    half = batch // 2
     width = cols * n_kv
     n_gates = gate_rows.shape[0]
 
-    count = itertools.count()
-
-    def load(src, dst):
-        copy = pltpu.make_async_copy(src, dst, load_sem.at[next(count)])
+    def load(number, src, dst):
+        copy = pltpu.make_async_copy(src, dst, load_sem.at[number])
         copy.start()
         return copy
 
     mine = gate_rows.at[:, pl.ds(pl.multiple_of(kv_index * cols, cols), cols)]
-    small = [
-        load(tokens, tok_v),
-        load(gain, gain_v),
-        load(w_query, wq_v),
-        load(mine, wg_v.at[pl.ds(0, n_gates)]),
-        load(mine, wg_v.at[pl.ds(64, n_gates)]),
-        load(w_key, wkv_v.at[pl.ds(0, head)]),
-        load(w_value, wkv_v.at[pl.ds(head, head)]),
-    ]
+    small = [load(0, tokens, tok_v), load(0, gain, gain_v), load(0, w_query, wq_v)]
+    small += [load(0, mine, wg_v.at[pl.ds(64 * k, n_gates)]) for k in range(4)]
+    small_new = [load(1, w_key, wkv_v.at[pl.ds(0, head)]), load(1, w_value, wkv_v.at[pl.ds(head, head)])]
 
     kv_offsets = [(a, b, 0) for a in range(n_kv0) for b in range(n_kv1) if a or b]
     tp_offsets = [(0, 0, c) for c in range(1, n_tp)]
     kv_offsets.sort(key=lambda o: -hops(o, sizes))
     tp_offsets.sort(key=lambda o: -hops(o, sizes))
 
+    def moved(p, o, n):
+        return jnp.where(p + o >= n, p + o - n, p + o) if o else p
+
     def peer(offset, sign=1):
-        return tuple(
-            lax.rem(p + (o if sign > 0 else n - o), n) if o else p for p, o, n in zip(at, offset, sizes)
-        )
+        return tuple(moved(p, o if sign > 0 else (n - o) % n, n) for p, o, n in zip(at, offset, sizes))
 
     barrier = pltpu.get_barrier_semaphore()
     for offset in kv_offsets + tp_offsets:
         pl.semaphore_signal(barrier, inc=1, device_id=peer(offset), device_id_type=MESH)
 
-    scalar_loads = [load(lengths, len_s), load(gate_bias, bias_s)]
-    cum_load = load(cum, cum_v)
-    block = batch // 8
-    first_cache = next(count)
-    for k in range(8):
-        pltpu.make_async_copy(
-            cache.at[pl.ds(k * block, block)],
-            cache_v.at[pl.ds(k * block, block)],
-            load_sem.at[first_cache + k],
-        ).start()
-    for k in range(7):
-        next(count)
-    wo_load = load(w_out, wo_v)
+    scalar_loads = [load(2, lengths, len_s), load(2, gate_bias, bias_s)]
+    cum_load = load(3, cum, cum_v)
+    blocks = 4
+    block = batch // blocks
+
+    def cache_copy(k):
+        part = pl.ds(k * block, block)
+        return pltpu.make_async_copy(cache.at[part], cache_v.at[part], load_sem.at[5 + k])
+
+    for k in range(blocks):
+        cache_copy(k).start()
+    wo_load = load(4, w_out, wo_v)
 
     numbers = itertools.count()
     sent = []
 
-    def slot(place, offsets):
-        return place[0] * n_kv1 + place[1] if offsets is kv_offsets else place[2]
-
     def exchange(buffer, offsets):
-        waits = []
+        number = next(numbers)
+        me = kv_index if offsets is kv_offsets else at[2]
         for offset in offsets:
-            number = next(numbers)
-            there, source = peer(offset), peer(offset, -1)
-            me, came = slot(at, offsets), slot(source, offsets)
-            out = pltpu.make_async_remote_copy(
+            pltpu.make_async_remote_copy(
                 src_ref=buffer.at[me],
                 dst_ref=buffer.at[me],
                 send_sem=send_sem.at[number],
                 recv_sem=recv_sem.at[number],
-                device_id=there,
+                device_id=peer(offset),
                 device_id_type=MESH,
-            )
-            out.start()
-            sent.append(out)
-            waits.append(
-                (
-                    came,
-                    pltpu.make_async_remote_copy(
-                        src_ref=buffer.at[came],
-                        dst_ref=buffer.at[came],
-                        send_sem=send_sem.at[number],
-                        recv_sem=recv_sem.at[number],
-                        device_id=source,
-                        device_id_type=MESH,
-                    ),
-                )
-            )
-        return waits[::-1]
-
-    wg_v[n_gates:64, :] = jnp.zeros((64 - n_gates, cols), bf16)
-    wg_v[64 + n_gates :, :] = jnp.zeros((64 - n_gates, cols), bf16)
-    for copy in small[:5]:
+            ).start()
+        others = buffer.at[pl.ds(0, len(offsets))]
+        every = pltpu.make_async_remote_copy(
+            src_ref=others,
+            dst_ref=others,
+            send_sem=send_sem.at[number],
+            recv_sem=recv_sem.at[number],
+            device_id=peer(offsets[0]),
+            device_id_type=MESH,
+        )
+        sent.append(every)
+        return every
+
+    for k in range(4):
+        wg_v[64 * k + n_gates : 64 * (k + 1), :] = jnp.zeros((64 - n_gates, cols), bf16)
+    for copy in small:
         copy.wait()
     tokens_f = tok_v[...].astype(f32)
     squares = jnp.sum(tokens_f * tokens_f, axis=1, keepdims=True)
     normed = (tokens_f * gain_v[...]).astype(bf16)
     lane = iota((batch, 128), 1)
-    half_lane = iota((half, 128), 1)
-    query_x[kv_index] = jnp.dot(normed, wq_v[...], preferred_element_type=f32).astype(bf16)
+    fold = batch // 4
+    fold_lane = iota((fold, 256), 1)
+    query_x[kv_index, :batch] = jnp.dot(normed, wq_v[...], preferred_element_type=f32).astype(bf16)
     part_gate = lax.dot_general(normed, wg_v[...], NT, preferred_element_type=f32)
-    part_gate = jnp.where(lane % 64 < n_gates, part_gate, squares)
-    gate_x[kv_index] = jnp.where(half_lane < 64, part_gate[:half], part_gate[half:]).astype(bf16)
+    part_gate = jnp.where(iota((batch, 256), 1) % 64 < n_gates, part_gate, squares)
+    folded = part_gate[:fold]
+    for k in range(1, 4):
+        folded = jnp.where(fold_lane >= 64 * k, part_gate[k * fold : (k + 1) * fold], folded)
+    query_x[kv_index, batch:] = folded.astype(bf16)
 
     pl.semaphore_wait(barrier, len(kv_offsets) + len(tp_offsets))
-    query_waits = exchange(query_x, kv_offsets)
-    gate_waits = exchange(gate_x, kv_offsets)
-    for copy in small[5:]:
+    query_all = exchange(query_x, kv_offsets)
+    for copy in small_new:
         copy.wait()
     new_x[kv_index] = lax.dot_general(normed, wkv_v[...], NT, preferred_element_type=f32).astype(bf16)
-    new_waits = exchange(new_x, kv_offsets)
+    new_all = exchange(new_x, kv_offsets)
 
     for copy in scalar_loads:
         copy.wait()
@@ -208,29 +192,29 @@
     holds = (length_col > 0) & (length_col <= span)
     holds = jnp.concatenate([jnp.where(holds, 1, 0)] * heads, axis=0) > 0
 
-    def flip(k, carry):
-        pltpu.make_async_copy(
-            cache.at[pl.ds(k * block, block)],
-            cache_v.at[pl.ds(k * block, block)],
-            load_sem.at[first_cache + k],
-        ).wait()
-        for j in range(block):
-            b = k * block + j
-            keys_t[pl.ds(pl.multiple_of(b * head, head), head), :] = cache_v[b].T[:head]
-        return carry
-
-    lax.fori_loop(0, 8, flip, 0)
-
-    sum_query = query_x[kv_index].astype(f32)
-    for came, wait in query_waits:
-        wait.wait_recv()
-        sum_query = sum_query + query_x[came].astype(f32)
-    gates = gate_x[kv_index].astype(f32)
-    for came, wait in gate_waits:
-        wait.wait_recv()
-        gates = gates + gate_x[came].astype(f32)
+    column = iota((4 * head, 2 * head), 1)
+    chosen = jnp.where(column < head, column + head, column + 2 * head)
+    chooser = jnp.where(iota((4 * head, 2 * head), 0) == chosen, 1.0, 0.0).astype(bf16)
+    for k in range(blocks):
+        cache_copy(k).wait()
+
+        def prepare(j, carry, k=k):
+            b = 2 * (k * block // 2 + j)
+            pair = jnp.concatenate([cache_v[b], cache_v[b + 1]], axis=1)
+            packed[k * block // 2 + j] = jnp.dot(pair, chooser, preferred_element_type=f32).astype(bf16)
+            for i in range(2):
+                keys_t[pl.ds(pl.multiple_of((b + i) * head, head), head), :] = cache_v[b + i].T[:head]
+            return carry
+
+        lax.fori_loop(0, block // 2, prepare, 0)
+
+    query_all.wait_recv()
+    total = query_x[0].astype(f32)
+    for k in range(1, n_kv):
+        total = total + query_x[k].astype(f32)
+    sum_query, gates = total[:batch], total[batch:]
     total_squares = jnp.concatenate(
-        [gates[:, n_gates : n_gates + 1], gates[:, 64 + n_gates : 65 + n_gates]], axis=0
+        [gates[:, 64 * k + n_gates : 64 * k + n_gates + 1] for k in range(4)], axis=0
     )
     row_scale = lax.rsqrt(total_squares / width + norm_eps)
     query = (row_scale * sum_query).astype(bf16).astype(f32)
@@ -239,8 +223,8 @@
         pick = at[2] * heads + h
         logit = jnp.concatenate(
             [
-                jnp.sum(jnp.where(half_lane == pick + 64 * part, gates, 0.0), axis=1, keepdims=True)
-                for part in range(2)
+                jnp.sum(jnp.where(fold_lane == pick + 64 * k, gates, 0.0), axis=1, keepdims=True)
+                for k in range(4)
             ],
             axis=0,
         )
@@ -273,10 +257,10 @@
         for k in range(tile // 128):
             peak = jnp.maximum(peak, score[:, k * 128 : (k + 1) * 128])
 
-    new_rows = new_x[kv_index].astype(f32)
-    for came, wait in new_waits:
-        wait.wait_recv()
-        new_rows = new_rows + new_x[came].astype(f32)
+    new_all.wait_recv()
+    new_rows = new_x[0].astype(f32)
+    for k in range(1, n_kv):
+        new_rows = new_rows + new_x[k].astype(f32)
     new_rows = (row_scale * new_rows).astype(bf16).astype(f32)
     new_rows = jnp.concatenate([new_rows] * heads, axis=0)
     new_biased = (
@@ -306,23 +290,20 @@
     stat_x[kv_index] = jnp.where(
         sub == 0, as_row(peak), jnp.where(sub == 1, as_row(weight_sum), as_row(anchor))
     )
-    stat_waits = exchange(stat_x, kv_offsets)
-
-    values = new_weight.astype(bf16).astype(f32) * new_rows
-    for p in range(batch // 2):
-        both = jnp.concatenate([cache_v[2 * p], cache_v[2 * p + 1]], axis=1)
-        out = jnp.dot(weights[...], both, preferred_element_type=f32)
-        values = (
-            values
-            + jnp.where(row_of == 2 * p, out[:, :128], 0.0)
-            + jnp.where(row_of == 2 * p + 1, out[:, 128:], 0.0)
-        )
-    val_x[kv_index] = values.T[head:].astype(bf16)
-    val_waits = exchange(val_x, kv_offsets)
+    stat_all = exchange(stat_x, kv_offsets)
+
+    values = jnp.where(lane_of < head, 0.0, new_weight.astype(bf16).astype(f32) * new_rows)
+    for q in range(batch // 4):
+        four = jnp.concatenate([packed[2 * q], packed[2 * q + 1]], axis=1)
+        out = jnp.dot(weights[...], four, preferred_element_type=f32)
+        for i in range(2):
+            values = values + jnp.where(row_of == 4 * q + 2 * i + side, out[:, 128 * i : 128 * (i + 1)], 0.0)
+    turned = values.T
+    val_x[kv_index] = (turned[:head] + turned[head:]).astype(bf16)
+    val_all = exchange(val_x, kv_offsets)
 
     wo_load.wait()
-    for _, wait in stat_waits:
-        wait.wait_recv()
+    stat_all.wait_recv()
     peaks = stat_x[:, 0, :]
     peak = jnp.max(peaks, axis=0, keepdims=True)
     factors = jnp.exp(peaks - peak)
@@ -330,8 +311,7 @@
     logs = peak + jnp.log(weight_sum) + jnp.sum(stat_x[:, 2, :], axis=0, keepdims=True)
     factors = factors / weight_sum
     log_weight[...] = jnp.concatenate([logs[:, h * batch : (h + 1) * batch] for h in range(heads)], axis=0)
-    for _, wait in val_waits:
-        wait.wait_recv()
+    val_all.wait_recv()
     acc = val_x[0].astype(f32) * factors[0:1]
     for k in range(1, n_kv):
         acc = acc + val_x[k].astype(f32) * factors[k : k + 1]
@@ -344,15 +324,24 @@
             preferred_element_type=f32,
         )
     out_x[at[2]] = part_out.astype(bf16)
-    out_waits = exchange(out_x, tp_offsets)
-    for _, wait in out_waits:
-        wait.wait_recv()
+    exchange(out_x, tp_offsets).wait_recv()
     acc = out_x[0].astype(f32)
     for k in range(1, n_tp):
         acc = acc + out_x[k].astype(f32)
     mixed[...] = acc.astype(bf16)
-    for out in sent:
-        out.wait_send()
+    for every in sent:
+        every.wait_send()
+
+
+def store(mixed, log_weight, mixed_out, log_out, sem):
+    copies = [
+        pltpu.make_async_copy(mixed, mixed_out, sem.at[0]),
+        pltpu.make_async_copy(log_weight, log_out, sem.at[1]),
+    ]
+    for copy in copies:
+        copy.start()
+    for copy in copies:
+        copy.wait()
 
 
 def shards(*args):
@@ -363,8 +352,6 @@
     span, head = cache.shape[1], cache.shape[3] // 2
     heads = cum.shape[1]
     rows = heads * batch
-    half = batch // 2
-    copies = 5 * (n_kv - 1) + n_tp - 1
     anywhere = pl.BlockSpec(memory_space=pl.ANY)
     near = pl.BlockSpec(memory_space=pltpu.VMEM)
     mixed, logs = pl.pallas_call(
@@ -380,25 +367,25 @@
             pltpu.VMEM((1, cols), f32),
             pltpu.VMEM(w_query.shape, bf16),
             pltpu.VMEM((2 * head, cols), bf16),
-            pltpu.VMEM((128, cols), bf16),
+            pltpu.VMEM((256, cols), bf16),
             pltpu.VMEM(w_out.shape, bf16),
             pltpu.SMEM(gate_bias.shape, f32),
             pltpu.SMEM(lengths.shape, jnp.int32),
             pltpu.VMEM((batch, span, 2 * head), bf16),
             pltpu.VMEM(cum.shape, f32),
             pltpu.VMEM((batch * head, span), bf16),
+            pltpu.VMEM((batch // 2, span, 2 * head), bf16),
             pltpu.VMEM((rows, span), f32),
             pltpu.VMEM((rows, span), f32),
             pltpu.VMEM((rows, span), bf16),
-            pltpu.VMEM((n_kv, batch, heads * head), bf16),
-            pltpu.VMEM((n_kv, half, 128), bf16),
+            pltpu.VMEM((n_kv, batch + batch // 4, heads * head), bf16),
             pltpu.VMEM((n_kv, batch, 2 * head), bf16),
             pltpu.VMEM((n_kv, head, rows), bf16),
             pltpu.VMEM((n_kv, 8, rows), f32),
             pltpu.VMEM((n_tp, batch, w_out.shape[1]), bf16),
-            pltpu.SemaphoreType.DMA((24,)),
-            pltpu.SemaphoreType.DMA((copies,)),
-            pltpu.SemaphoreType.DMA((copies,)),
+            pltpu.SemaphoreType.DMA((9,)),
+            pltpu.SemaphoreType.DMA((5,)),
+            pltpu.SemaphoreType.DMA((5,)),
         ],
         compiler_params=pltpu.CompilerParams(
             collective_id=0, has_side_effects=True, vmem_limit_bytes=60 * 1024 * 1024
@@ -416,6 +403,14 @@
         lengths,
         w_out,
     )
+    mixed, logs = pl.pallas_call(
+        store,
+        out_shape=(jax.ShapeDtypeStruct(mixed.shape, bf16), jax.ShapeDtypeStruct(logs.shape, f32)),
+        in_specs=(near, near),
+        out_specs=(anywhere, anywhere),
+        scratch_shapes=[pltpu.SemaphoreType.DMA((2,))],
+        compiler_params=pltpu.CompilerParams(vmem_limit_bytes=1024 * 1024),
+    )(mixed, logs)
     return mixed, logs.T
 
 

time: 32.4 us -> 29.4 us (0.907)
  Pallas kernels: 30.4 us -> 28.7 us
  local copies, waits for them, and re-layouts: 1.19 us -> 0 us
    pallas_call x1, Pallas kernels: 30.4 us -> 28.1 us  [shards(): pl.pallas_call(functools.partial(kernel, n_kv0, n_kv1, n_tp), out_shape=(...]
    unnamed x2 -> x0, local copies, waits for them, and re-layouts: 1.19 us -> none
    pallas_call x0 -> x1, Pallas kernels: none -> 0.63 us  [shards(): pl.pallas_call(store, out_shape=(jax.ShapeDtypeStruct(mixed.shape, bf16),...]
where the time goes in v3:
time: 29.4 us; the launch traced here: 29.3 us
  Pallas kernels  28.7 us (98%)
  between operations  0.64 us (2%)
    pallas_call x1, Pallas kernels, shards(): pl.pallas_call(functools.partial(kernel, n_kv0, n_kv1, n_tp), out_shape=(...  28.1 us
    pallas_call x1, Pallas kernels, shards(): pl.pallas_call(store, out_shape=(jax.ShapeDtypeStruct(mixed.shape, bf16),...  0.63 us

profile of v3, /device:TPU:1, one launch (start us, length us, event | category | flops | bytes accessed | tf_op | source)
XLA Modules:
  0.0 29.3 jit_solution(5618479379109478839)
XLA Ops:
  0.6 28.1 %shard_map.122 = (bf16[32,256]{1,0:T(8,128)(2,1)S(1)}, f32[4,32]{1,0:T(4,128)S(1)}) custom-call(bf16[32,256]{1,0:T(8,128)(2,1)} %tokens.1, f32[1,256]{1,0:T(1,128)} %bitcast.10, bf16[256,256]{1,0:T(8,128)(2,1)} %w_query.1, bf16[64,256]{1,0:T(8,128)(2,1)} %bitcast.8, bf16[64,256]{1,0:T(8,128)(2,1)} %bitcast.9, bf16[32,4096]{1,0:T(8,128)(2,1)} %bitcast.7, ...), custom_call_target="tpu_custom_call" | custom-call | tf_op jit(solution)/shard_map/pallas_call | solution.py:357
  28.7 0.6 %shard_map.123 = (bf16[32,256]{1,0:T(8,128)(2,1)}, f32[4,32]{1,0:T(4,128)}) custom-call(bf16[32,256]{1,0:T(8,128)(2,1)S(1)} %get-tuple-element.6.mixed, f32[4,32]{1,0:T(4,128)S(1)} %get-tuple-element.7.log_weight), custom_call_target="tpu_custom_call" | custom-call | tf_op jit(solution)/shard_map/pallas_call | solution.py:406

commit v4 on v3

--- a/solution.py
+++ b/solution.py
@@ -15,6 +15,7 @@
 norm_eps = 1e-05
 masked_floor = -1e30
 empty_peak = -1e29
+EARLY = 1
 f32, bf16 = jnp.float32, jnp.bfloat16
 
 
@@ -58,8 +59,10 @@
     cum_neg,
     biased,
     weights,
-    query_x,
-    new_x,
+    query_1,
+    query_2,
+    new_1,
+    new_2,
     val_x,
     stat_x,
     out_x,
@@ -84,25 +87,27 @@
         copy.start()
         return copy
 
+    kv_offsets = [(a, b, 0) for a in range(n_kv0) for b in range(n_kv1) if a or b]
+    tp_offsets = [(0, 0, c) for c in range(1, n_tp)]
+    axis_offsets = ([(a, 0, 0) for a in range(1, n_kv0)], [(0, b, 0) for b in range(1, n_kv1)])
+    for offsets in (kv_offsets, tp_offsets, *axis_offsets):
+        offsets.sort(key=lambda o: (-hops(o, sizes), -sum(1 for c in o if c)))
+
+    def moved(p, o, n):
+        return jnp.where(p + o >= n, p + o - n, p + o) if o else p
+
+    def peer(offset, sign=1):
+        return tuple(moved(p, o if sign > 0 else (n - o) % n, n) for p, o, n in zip(at, offset, sizes))
+
+    barrier = pltpu.get_barrier_semaphore()
+    near_offsets = axis_offsets[0] + axis_offsets[1] + tp_offsets
+    for offset in near_offsets:
+        pl.semaphore_signal(barrier, inc=1, device_id=peer(offset), device_id_type=MESH)
+
     mine = gate_rows.at[:, pl.ds(pl.multiple_of(kv_index * cols, cols), cols)]
     small = [load(0, tokens, tok_v), load(0, gain, gain_v), load(0, w_query, wq_v)]
-    small += [load(0, mine, wg_v.at[pl.ds(64 * k, n_gates)]) for k in range(4)]
+    small += [load(0, mine, wg_v.at[pl.ds(0, n_gates)])]
     small_new = [load(1, w_key, wkv_v.at[pl.ds(0, head)]), load(1, w_value, wkv_v.at[pl.ds(head, head)])]
-
-    kv_offsets = [(a, b, 0) for a in range(n_kv0) for b in range(n_kv1) if a or b]
-    tp_offsets = [(0, 0, c) for c in range(1, n_tp)]
-    kv_offsets.sort(key=lambda o: -hops(o, sizes))
-    tp_offsets.sort(key=lambda o: -hops(o, sizes))
-
-    def moved(p, o, n):
-        return jnp.where(p + o >= n, p + o - n, p + o) if o else p
-
-    def peer(offset, sign=1):
-        return tuple(moved(p, o if sign > 0 else (n - o) % n, n) for p, o, n in zip(at, offset, sizes))
-
-    barrier = pltpu.get_barrier_semaphore()
-    for offset in kv_offsets + tp_offsets:
-        pl.semaphore_signal(barrier, inc=1, device_id=peer(offset), device_id_type=MESH)
 
     scalar_loads = [load(2, lengths, len_s), load(2, gate_bias, bias_s)]
     cum_load = load(3, cum, cum_v)
@@ -120,54 +125,67 @@
     numbers = itertools.count()
     sent = []
 
-    def exchange(buffer, offsets):
+    def exchange(buffer, *ways):
         number = next(numbers)
-        me = kv_index if offsets is kv_offsets else at[2]
-        for offset in offsets:
-            pltpu.make_async_remote_copy(
-                src_ref=buffer.at[me],
-                dst_ref=buffer.at[me],
-                send_sem=send_sem.at[number],
-                recv_sem=recv_sem.at[number],
-                device_id=peer(offset),
-                device_id_type=MESH,
-            ).start()
-        others = buffer.at[pl.ds(0, len(offsets))]
+        copies = 0
+        for me, offsets in ways:
+            for offset in offsets:
+                copies += 1
+                pltpu.make_async_remote_copy(
+                    src_ref=buffer.at[me],
+                    dst_ref=buffer.at[me],
+                    send_sem=send_sem.at[number],
+                    recv_sem=recv_sem.at[number],
+                    device_id=peer(offset),
+                    device_id_type=MESH,
+                ).start()
+        others = buffer.at[pl.ds(0, copies)]
         every = pltpu.make_async_remote_copy(
             src_ref=others,
             dst_ref=others,
             send_sem=send_sem.at[number],
             recv_sem=recv_sem.at[number],
-            device_id=peer(offsets[0]),
+            device_id=peer(ways[0][1][0]),
             device_id_type=MESH,
         )
         sent.append(every)
         return every
 
-    for k in range(4):
-        wg_v[64 * k + n_gates : 64 * (k + 1), :] = jnp.zeros((64 - n_gates, cols), bf16)
+    first_slots = (at[1], n_kv1 + at[0])
+    first_ways = tuple(zip(first_slots, (axis_offsets[1], axis_offsets[0])))
+    second_slots = (at[0], n_kv0 + at[1])
+    second_ways = tuple(zip(second_slots, axis_offsets))
+
+    def total(buffer, low, high):
+        acc = buffer[low].astype(f32)
+        for k in range(low + 1, high):
+            acc = acc + buffer[k].astype(f32)
+        return acc
+
+    wg_v[n_gates:, :] = jnp.zeros((wg_v.shape[0] - n_gates, cols), bf16)
     for copy in small:
         copy.wait()
     tokens_f = tok_v[...].astype(f32)
     squares = jnp.sum(tokens_f * tokens_f, axis=1, keepdims=True)
     normed = (tokens_f * gain_v[...]).astype(bf16)
     lane = iota((batch, 128), 1)
-    fold = batch // 4
-    fold_lane = iota((fold, 256), 1)
-    query_x[kv_index, :batch] = jnp.dot(normed, wq_v[...], preferred_element_type=f32).astype(bf16)
+    half = batch // 2
+    part_query = jnp.dot(normed, wq_v[...], preferred_element_type=f32).astype(bf16)
     part_gate = lax.dot_general(normed, wg_v[...], NT, preferred_element_type=f32)
-    part_gate = jnp.where(iota((batch, 256), 1) % 64 < n_gates, part_gate, squares)
-    folded = part_gate[:fold]
-    for k in range(1, 4):
-        folded = jnp.where(fold_lane >= 64 * k, part_gate[k * fold : (k + 1) * fold], folded)
-    query_x[kv_index, batch:] = folded.astype(bf16)
-
-    pl.semaphore_wait(barrier, len(kv_offsets) + len(tp_offsets))
-    query_all = exchange(query_x, kv_offsets)
+    part_gate = jnp.where(lane < n_gates, part_gate, squares).astype(bf16)
+    for part in range(2):
+        chunk = slice(part * half, (part + 1) * half)
+        query_1[first_slots[part], :, : heads * head] = part_query[chunk]
+        query_1[first_slots[part], :, heads * head :] = part_gate[chunk]
+
+    pl.semaphore_wait(barrier, len(near_offsets))
+    query_all = exchange(query_1, *first_ways)
     for copy in small_new:
         copy.wait()
-    new_x[kv_index] = lax.dot_general(normed, wkv_v[...], NT, preferred_element_type=f32).astype(bf16)
-    new_all = exchange(new_x, kv_offsets)
+    part_new = lax.dot_general(normed, wkv_v[...], NT, preferred_element_type=f32).astype(bf16)
+    for part in range(2):
+        new_1[first_slots[part]] = part_new[part * half : (part + 1) * half]
+    new_all = exchange(new_1, *first_ways)
 
     for copy in scalar_loads:
         copy.wait()
@@ -195,10 +213,11 @@
     column = iota((4 * head, 2 * head), 1)
     chosen = jnp.where(column < head, column + head, column + 2 * head)
     chooser = jnp.where(iota((4 * head, 2 * head), 0) == chosen, 1.0, 0.0).astype(bf16)
-    for k in range(blocks):
+
+    def prepare(k):
         cache_copy(k).wait()
 
-        def prepare(j, carry, k=k):
+        def one(j, carry):
             b = 2 * (k * block // 2 + j)
             pair = jnp.concatenate([cache_v[b], cache_v[b + 1]], axis=1)
             packed[k * block // 2 + j] = jnp.dot(pair, chooser, preferred_element_type=f32).astype(bf16)
@@ -206,28 +225,32 @@
                 keys_t[pl.ds(pl.multiple_of((b + i) * head, head), head), :] = cache_v[b + i].T[:head]
             return carry
 
-        lax.fori_loop(0, block // 2, prepare, 0)
+        for j in range(block//2): one(j,0)
+
+    for k in range(EARLY):
+        prepare(k)
 
     query_all.wait_recv()
-    total = query_x[0].astype(f32)
-    for k in range(1, n_kv):
-        total = total + query_x[k].astype(f32)
-    sum_query, gates = total[:batch], total[batch:]
-    total_squares = jnp.concatenate(
-        [gates[:, 64 * k + n_gates : 64 * k + n_gates + 1] for k in range(4)], axis=0
-    )
+    query_2[second_slots[0]] = total(query_1, 0, n_kv1).astype(bf16)
+    query_2[second_slots[1]] = total(query_1, n_kv1, n_kv1 + n_kv0).astype(bf16)
+    query_all = exchange(query_2, *second_ways)
+    new_all.wait_recv()
+    new_2[second_slots[0]] = total(new_1, 0, n_kv1).astype(bf16)
+    new_2[second_slots[1]] = total(new_1, n_kv1, n_kv1 + n_kv0).astype(bf16)
+    new_all = exchange(new_2, *second_ways)
+    for k in range(EARLY, blocks):
+        prepare(k)
+    query_all.wait_recv()
+    new_all.wait_recv()
+    sums = jnp.concatenate([total(query_2, 0, n_kv0), total(query_2, n_kv0, n_kv0 + n_kv1)], axis=0)
+    sum_query, gates = sums[:, : heads * head], sums[:, heads * head :]
+    total_squares = gates[:, n_gates : n_gates + 1]
     row_scale = lax.rsqrt(total_squares / width + norm_eps)
     query = (row_scale * sum_query).astype(bf16).astype(f32)
     log_gate = []
     for h in range(heads):
         pick = at[2] * heads + h
-        logit = jnp.concatenate(
-            [
-                jnp.sum(jnp.where(fold_lane == pick + 64 * k, gates, 0.0), axis=1, keepdims=True)
-                for k in range(4)
-            ],
-            axis=0,
-        )
+        logit = jnp.sum(jnp.where(lane == pick, gates, 0.0), axis=1, keepdims=True)
         logit = row_scale * logit + bias_s[h]
         log_gate.append(jnp.minimum(logit, 0.0) - jnp.log1p(jnp.exp(-jnp.abs(logit))))
     cum_query = last_cum + jnp.concatenate(log_gate, axis=0)
@@ -257,10 +280,7 @@
         for k in range(tile // 128):
             peak = jnp.maximum(peak, score[:, k * 128 : (k + 1) * 128])
 
-    new_all.wait_recv()
-    new_rows = new_x[0].astype(f32)
-    for k in range(1, n_kv):
-        new_rows = new_rows + new_x[k].astype(f32)
+    new_rows = jnp.concatenate([total(new_2, 0, n_kv0), total(new_2, n_kv0, n_kv0 + n_kv1)], axis=0)
     new_rows = (row_scale * new_rows).astype(bf16).astype(f32)
     new_rows = jnp.concatenate([new_rows] * heads, axis=0)
     new_biased = (
@@ -285,12 +305,12 @@
     def as_row(column):
         return jnp.sum(jnp.where(diagonal, column, 0.0), axis=0, keepdims=True)
 
-    sub = iota((8, 128), 0)
+    sub = iota((4, 128), 0)
     anchor = jnp.where(holds, cum_query, 0.0)
     stat_x[kv_index] = jnp.where(
         sub == 0, as_row(peak), jnp.where(sub == 1, as_row(weight_sum), as_row(anchor))
     )
-    stat_all = exchange(stat_x, kv_offsets)
+    stat_all = exchange(stat_x, (kv_index, kv_offsets))
 
     values = jnp.where(lane_of < head, 0.0, new_weight.astype(bf16).astype(f32) * new_rows)
     for q in range(batch // 4):
@@ -300,7 +320,7 @@
             values = values + jnp.where(row_of == 4 * q + 2 * i + side, out[:, 128 * i : 128 * (i + 1)], 0.0)
     turned = values.T
     val_x[kv_index] = (turned[:head] + turned[head:]).astype(bf16)
-    val_all = exchange(val_x, kv_offsets)
+    val_all = exchange(val_x, (kv_index, kv_offsets))
 
     wo_load.wait()
     stat_all.wait_recv()
@@ -324,7 +344,7 @@
             preferred_element_type=f32,
         )
     out_x[at[2]] = part_out.astype(bf16)
-    exchange(out_x, tp_offsets).wait_recv()
+    exchange(out_x, (at[2], tp_offsets)).wait_recv()
     acc = out_x[0].astype(f32)
     for k in range(1, n_tp):
         acc = acc + out_x[k].astype(f32)
@@ -352,6 +372,7 @@
     span, head = cache.shape[1], cache.shape[3] // 2
     heads = cum.shape[1]
     rows = heads * batch
+    half = batch // 2
     anywhere = pl.BlockSpec(memory_space=pl.ANY)
     near = pl.BlockSpec(memory_space=pltpu.VMEM)
     mixed, logs = pl.pallas_call(
@@ -367,7 +388,7 @@
             pltpu.VMEM((1, cols), f32),
             pltpu.VMEM(w_query.shape, bf16),
             pltpu.VMEM((2 * head, cols), bf16),
-            pltpu.VMEM((256, cols), bf16),
+            pltpu.VMEM((128, cols), bf16),
             pltpu.VMEM(w_out.shape, bf16),
             pltpu.SMEM(gate_bias.shape, f32),
             pltpu.SMEM(lengths.shape, jnp.int32),
@@ -378,14 +399,16 @@
             pltpu.VMEM((rows, span), f32),
             pltpu.VMEM((rows, span), f32),
             pltpu.VMEM((rows, span), bf16),
-            pltpu.VMEM((n_kv, batch + batch // 4, heads * head), bf16),
-            pltpu.VMEM((n_kv, batch, 2 * head), bf16),
+            pltpu.VMEM((n_kv0 + n_kv1, half, heads * head + 128), bf16),
+            pltpu.VMEM((n_kv0 + n_kv1, half, heads * head + 128), bf16),
+            pltpu.VMEM((n_kv0 + n_kv1, half, 2 * head), bf16),
+            pltpu.VMEM((n_kv0 + n_kv1, half, 2 * head), bf16),
             pltpu.VMEM((n_kv, head, rows), bf16),
-            pltpu.VMEM((n_kv, 8, rows), f32),
+            pltpu.VMEM((n_kv, 4, rows), f32),
             pltpu.VMEM((n_tp, batch, w_out.shape[1]), bf16),
             pltpu.SemaphoreType.DMA((9,)),
-            pltpu.SemaphoreType.DMA((5,)),
-            pltpu.SemaphoreType.DMA((5,)),
+            pltpu.SemaphoreType.DMA((7,)),
+            pltpu.SemaphoreType.DMA((7,)),
         ],
         compiler_params=pltpu.CompilerParams(
             collective_id=0, has_side_effects=True, vmem_limit_bytes=60 * 1024 * 1024

time: 29.4 us -> 28 us (0.952)
  Pallas kernels: 28.7 us -> 27.2 us
    pallas_call x1, Pallas kernels: 28.1 us -> 26.6 us  [shards(): pl.pallas_call(functools.partial(kernel, n_kv0, n_kv1, n_tp), out_shape=(...]
where the time goes in v4:
time: 28 us; the launch traced here: 27.9 us
  Pallas kernels  27.2 us (97%)
  between operations  0.64 us (2%)
    pallas_call x1, Pallas kernels, shards(): pl.pallas_call(functools.partial(kernel, n_kv0, n_kv1, n_tp), out_shape=(...  26.6 us
    pallas_call x1, Pallas kernels, shards(): pl.pallas_call(store, out_shape=(jax.ShapeDtypeStruct(mixed.shape, bf16),...  0.63 us

profile of v4, /device:TPU:1, one launch (start us, length us, event | category | flops | bytes accessed | tf_op | source)
XLA Modules:
  0.0 27.9 jit_solution(6163004714271528888)
XLA Ops:
  0.6 26.6 %shard_map.122 = (bf16[32,256]{1,0:T(8,128)(2,1)S(1)}, f32[4,32]{1,0:T(4,128)S(1)}) custom-call(bf16[32,256]{1,0:T(8,128)(2,1)} %tokens.1, f32[1,256]{1,0:T(1,128)} %bitcast.10, bf16[256,256]{1,0:T(8,128)(2,1)} %w_query.1, bf16[64,256]{1,0:T(8,128)(2,1)} %bitcast.8, bf16[64,256]{1,0:T(8,128)(2,1)} %bitcast.9, bf16[32,4096]{1,0:T(8,128)(2,1)} %bitcast.7, ...), custom_call_target="tpu_custom_call" | custom-call | tf_op jit(solution)/shard_map/pallas_call | solution.py:378
  27.2 0.6 %shard_map.123 = (bf16[32,256]{1,0:T(8,128)(2,1)}, f32[4,32]{1,0:T(4,128)}) custom-call(bf16[32,256]{1,0:T(8,128)(2,1)S(1)} %get-tuple-element.6.mixed, f32[4,32]{1,0:T(4,128)S(1)} %get-tuple-element.7.log_weight), custom_call_target="tpu_custom_call" | custom-call | tf_op jit(solution)/shard_map/pallas_call | solution.py:429

commit v5 on v4

--- a/solution.py
+++ b/solution.py
@@ -15,6 +15,7 @@
 norm_eps = 1e-05
 masked_floor = -1e30
 empty_peak = -1e29
+MID, SEND = 2, 6
 EARLY = 1
 f32, bf16 = jnp.float32, jnp.bfloat16
 
@@ -65,6 +66,7 @@
     new_2,
     val_x,
     stat_x,
+    scale,
     out_x,
     load_sem,
     send_sem,
@@ -271,7 +273,7 @@
         [jnp.where(row_of == 2 * p + side, scaled, 0.0).astype(bf16) for p in range(batch // 2)], axis=1
     )
 
-    tile = 256
+    tile = 640
     peak = jnp.full((rows, 128), masked_floor, f32)
     for n in range(span // tile):
         cut = slice(n * tile, (n + 1) * tile)
@@ -300,6 +302,20 @@
     new_weight = jnp.where(holds, jnp.exp(new_biased - peak), 0.0)
     weight_sum = jnp.sum(sums, axis=1, keepdims=True) + new_weight
 
+    values = jnp.where(lane_of < head, 0.0, new_weight.astype(bf16).astype(f32) * new_rows)
+
+    def weigh(values, first, count):
+        wide = jnp.concatenate([packed[2 * first + i] for i in range(2 * count)], axis=1)
+        out = jnp.dot(weights[...], wide, preferred_element_type=f32)
+        for i in range(2 * count):
+            pair = 4 * first + 2 * i
+            values = values + jnp.where(row_of == pair + side, out[:, 128 * i : 128 * (i + 1)], 0.0)
+        return values
+
+    quads = batch // 4
+    for q in range(0, MID):
+        values = weigh(values, q, 1)
+
     diagonal = iota((rows, 128), 0) == lane_of
 
     def as_row(column):
@@ -312,15 +328,30 @@
     )
     stat_all = exchange(stat_x, (kv_index, kv_offsets))
 
-    values = jnp.where(lane_of < head, 0.0, new_weight.astype(bf16).astype(f32) * new_rows)
-    for q in range(batch // 4):
-        four = jnp.concatenate([packed[2 * q], packed[2 * q + 1]], axis=1)
-        out = jnp.dot(weights[...], four, preferred_element_type=f32)
-        for i in range(2):
-            values = values + jnp.where(row_of == 4 * q + 2 * i + side, out[:, 128 * i : 128 * (i + 1)], 0.0)
-    turned = values.T
-    val_x[kv_index] = (turned[:head] + turned[head:]).astype(bf16)
-    val_all = exchange(val_x, (kv_index, kv_offsets))
+
+    for q in range(MID, quads // 2):
+        values = weigh(values, q, 1)
+
+    half_lane = iota((half, 128), 1)
+
+    def paired(column, part):
+        found = []
+        for h in range(0, heads, 2):
+            low, high = h * batch + part * half, (h + 1) * batch + part * half
+            found.append(jnp.where(half_lane < head, column[low : low + half], column[high : high + half]))
+        return jnp.concatenate(found, axis=0)
+
+    def fold(values):
+        return values + pltpu.roll(values, head, 1)
+
+    val_x[0, kv_index] = paired(fold(values), 0).astype(bf16)
+    for q in range(quads // 2, SEND):
+        values = weigh(values, q, 1)
+    val_all = [exchange(val_x.at[0], (kv_index, kv_offsets))]
+    for q in range(SEND, quads):
+        values = weigh(values, q, 1)
+    val_x[1, kv_index] = paired(fold(values), 1).astype(bf16)
+    val_all.append(exchange(val_x.at[1], (kv_index, kv_offsets)))
 
     wo_load.wait()
     stat_all.wait_recv()
@@ -331,24 +362,26 @@
     logs = peak + jnp.log(weight_sum) + jnp.sum(stat_x[:, 2, :], axis=0, keepdims=True)
     factors = factors / weight_sum
     log_weight[...] = jnp.concatenate([logs[:, h * batch : (h + 1) * batch] for h in range(heads)], axis=0)
-    val_all.wait_recv()
-    acc = val_x[0].astype(f32) * factors[0:1]
-    for k in range(1, n_kv):
-        acc = acc + val_x[k].astype(f32) * factors[k : k + 1]
-    attended = acc.T.astype(bf16)
-    part_out = jnp.zeros((batch, w_out.shape[1]), f32)
-    for h in range(heads):
-        part_out = part_out + jnp.dot(
-            attended[h * batch : (h + 1) * batch],
-            wo_v[h * head : (h + 1) * head],
-            preferred_element_type=f32,
-        )
-    out_x[at[2]] = part_out.astype(bf16)
-    exchange(out_x, (at[2], tp_offsets)).wait_recv()
-    acc = out_x[0].astype(f32)
-    for k in range(1, n_tp):
-        acc = acc + out_x[k].astype(f32)
-    mixed[...] = acc.astype(bf16)
+    columns = factors.T
+    for part in range(2):
+        for k in range(n_kv):
+            scale[part, k] = paired(columns[:, k : k + 1], part)
+    out_all = []
+    for part in range(2):
+        val_all[part].wait_recv()
+        acc = val_x[part, 0].astype(f32) * scale[part, 0]
+        for k in range(1, n_kv):
+            acc = acc + val_x[part, k].astype(f32) * scale[part, k]
+        attended = jnp.concatenate([acc[i * half : (i + 1) * half] for i in range(heads // 2)], axis=1)
+        part_out = jnp.dot(attended.astype(bf16), wo_v[...], preferred_element_type=f32)
+        out_x[part, at[2]] = part_out.astype(bf16)
+        out_all.append(exchange(out_x.at[part], (at[2], tp_offsets)))
+    for part in range(2):
+        out_all[part].wait_recv()
+        acc = out_x[part, 0].astype(f32)
+        for k in range(1, n_tp):
+            acc = acc + out_x[part, k].astype(f32)
+        mixed[part * half : (part + 1) * half] = acc.astype(bf16)
     for every in sent:
         every.wait_send()
 
@@ -403,12 +436,13 @@
             pltpu.VMEM((n_kv0 + n_kv1, half, heads * head + 128), bf16),
             pltpu.VMEM((n_kv0 + n_kv1, half, 2 * head), bf16),
             pltpu.VMEM((n_kv0 + n_kv1, half, 2 * head), bf16),
-            pltpu.VMEM((n_kv, head, rows), bf16),
+            pltpu.VMEM((2, n_kv, rows // 4, 2 * head), bf16),
             pltpu.VMEM((n_kv, 4, rows), f32),
-            pltpu.VMEM((n_tp, batch, w_out.shape[1]), bf16),
+            pltpu.VMEM((2, n_kv, rows // 4, 2 * head), f32),
+            pltpu.VMEM((2, n_tp, half, w_out.shape[1]), bf16),
             pltpu.SemaphoreType.DMA((9,)),
-            pltpu.SemaphoreType.DMA((7,)),
-            pltpu.SemaphoreType.DMA((7,)),
+            pltpu.SemaphoreType.DMA((9,)),
+            pltpu.SemaphoreType.DMA((9,)),
         ],
         compiler_params=pltpu.CompilerParams(
             collective_id=0, has_side_effects=True, vmem_limit_bytes=60 * 1024 * 1024

time: 28 us -> 27.3 us (0.975)
  Pallas kernels: 27.2 us -> 26.6 us
    pallas_call x1, Pallas kernels: 26.6 us -> 25.9 us  [shards(): pl.pallas_call(functools.partial(kernel, n_kv0, n_kv1, n_tp), out_shape=(...]
where the time goes in v5:
time: 27.3 us; the launch traced here: 27.2 us
  Pallas kernels  26.6 us (97%)
  between operations  0.64 us (2%)
    pallas_call x1, Pallas kernels, shards(): pl.pallas_call(functools.partial(kernel, n_kv0, n_kv1, n_tp), out_shape=(...  25.9 us
    pallas_call x1, Pallas kernels, shards(): pl.pallas_call(store, out_shape=(jax.ShapeDtypeStruct(mixed.shape, bf16),...  0.63 us

profile of v5, /device:TPU:1, one launch (start us, length us, event | category | flops | bytes accessed | tf_op | source)
XLA Modules:
  0.0 27.2 jit_solution(13192806349876911569)
XLA Ops:
  0.6 25.9 %shard_map.122 = (bf16[32,256]{1,0:T(8,128)(2,1)S(1)}, f32[4,32]{1,0:T(4,128)S(1)}) custom-call(bf16[32,256]{1,0:T(8,128)(2,1)} %tokens.1, f32[1,256]{1,0:T(1,128)} %bitcast.10, bf16[256,256]{1,0:T(8,128)(2,1)} %w_query.1, bf16[64,256]{1,0:T(8,128)(2,1)} %bitcast.8, bf16[64,256]{1,0:T(8,128)(2,1)} %bitcast.9, bf16[32,4096]{1,0:T(8,128)(2,1)} %bitcast.7, ...), custom_call_target="tpu_custom_call" | custom-call | tf_op jit(solution)/shard_map/pallas_call | solution.py:411
  26.6 0.6 %shard_map.123 = (bf16[32,256]{1,0:T(8,128)(2,1)}, f32[4,32]{1,0:T(4,128)}) custom-call(bf16[32,256]{1,0:T(8,128)(2,1)S(1)} %get-tuple-element.6.mixed, f32[4,32]{1,0:T(4,128)S(1)} %get-tuple-element.7.log_weight), custom_call_target="tpu_custom_call" | custom-call | tf_op jit(solution)/shard_map/pallas_call | solution.py:463

commit v6 on v5

--- a/solution.py
+++ b/solution.py
@@ -15,7 +15,9 @@
 norm_eps = 1e-05
 masked_floor = -1e30
 empty_peak = -1e29
-MID, SEND = 2, 6
+SEGMENTS = ((0, 512), (512, 1024), (1024, 1280))
+WIDEST = 640
+MID, SEND = 4, 6
 EARLY = 1
 f32, bf16 = jnp.float32, jnp.bfloat16
 
@@ -26,6 +28,12 @@
 
 def hops(offset, sizes):
     return sum(min(o, n - o) for o, n in zip(offset, sizes))
+
+
+def cuts(low, high):
+    steps = -(-(high - low) // WIDEST)
+    step = -(-(high - low) // steps // 128) * 128
+    return [slice(k, min(k + step, high)) for k in range(low, high, step)]
 
 
 def kernel(
@@ -103,6 +111,7 @@
 
     barrier = pltpu.get_barrier_semaphore()
     near_offsets = axis_offsets[0] + axis_offsets[1] + tp_offsets
+    near_offsets.sort(key=lambda o: -hops(o, sizes))
     for offset in near_offsets:
         pl.semaphore_signal(barrier, inc=1, device_id=peer(offset), device_id_type=MESH)
 
@@ -273,14 +282,22 @@
         [jnp.where(row_of == 2 * p + side, scaled, 0.0).astype(bf16) for p in range(batch // 2)], axis=1
     )
 
-    tile = 640
-    peak = jnp.full((rows, 128), masked_floor, f32)
-    for n in range(span // tile):
-        cut = slice(n * tile, (n + 1) * tile)
-        score = jnp.dot(spread, keys_t[:, cut], preferred_element_type=f32) + cum_neg[:, cut]
-        biased[:, cut] = score
-        for k in range(tile // 128):
-            peak = jnp.maximum(peak, score[:, k * 128 : (k + 1) * 128])
+    peaks, sums = [], []
+    for low, high in SEGMENTS:
+        top = jnp.full((rows, 128), masked_floor, f32)
+        for cut in cuts(low, high):
+            score = jnp.dot(spread, keys_t[:, cut], preferred_element_type=f32) + cum_neg[:, cut]
+            biased[:, cut] = score
+            for k in range(score.shape[1] // 128):
+                top = jnp.maximum(top, score[:, k * 128 : (k + 1) * 128])
+        top = jnp.maximum(jnp.max(top, axis=1, keepdims=True), empty_peak)
+        part_sum = jnp.zeros((rows, 128), f32)
+        for k in range(low, high, 128):
+            weight = jnp.exp(biased[:, k : k + 128] - top)
+            part_sum = part_sum + weight
+            weights[:, k : k + 128] = weight.astype(bf16)
+        peaks.append(top)
+        sums.append(jnp.sum(part_sum, axis=1, keepdims=True))
 
     new_rows = jnp.concatenate([total(new_2, 0, n_kv0), total(new_2, n_kv0, n_kv0 + n_kv1)], axis=0)
     new_rows = (row_scale * new_rows).astype(bf16).astype(f32)
@@ -290,31 +307,37 @@
         - cum_query
     )
 
-    peak = jnp.max(peak, axis=1, keepdims=True)
+    peak = functools.reduce(jnp.maximum, peaks)
     peak = jnp.where(holds, jnp.maximum(peak, new_biased), peak)
-    peak = jnp.maximum(peak, empty_peak)
-    sums = jnp.zeros((rows, 128), f32)
-    for n in range(span // 128):
-        cut = slice(n * 128, (n + 1) * 128)
-        weight = jnp.exp(biased[:, cut] - peak)
-        sums = sums + weight
-        weights[:, cut] = weight.astype(bf16)
+    shrink = [jnp.exp(p - peak) for p in peaks]
     new_weight = jnp.where(holds, jnp.exp(new_biased - peak), 0.0)
-    weight_sum = jnp.sum(sums, axis=1, keepdims=True) + new_weight
-
-    values = jnp.where(lane_of < head, 0.0, new_weight.astype(bf16).astype(f32) * new_rows)
-
-    def weigh(values, first, count):
-        wide = jnp.concatenate([packed[2 * first + i] for i in range(2 * count)], axis=1)
-        out = jnp.dot(weights[...], wide, preferred_element_type=f32)
-        for i in range(2 * count):
-            pair = 4 * first + 2 * i
-            values = values + jnp.where(row_of == pair + side, out[:, 128 * i : 128 * (i + 1)], 0.0)
-        return values
+    weight_sum = sum(s * f for s, f in zip(sums, shrink)) + new_weight
+
+    found = [jnp.zeros((rows, 128), f32) for _ in SEGMENTS]
+
+    def weigh(segment, q):
+        low, high = SEGMENTS[segment]
+        four = jnp.concatenate([packed[2 * q + i, low:high] for i in range(2)], axis=1)
+        out = jnp.dot(weights[:, low:high], four, preferred_element_type=f32)
+        for i in range(2):
+            pair = 4 * q + 2 * i
+            found[segment] = found[segment] + jnp.where(
+                row_of == pair + side, out[:, 128 * i : 128 * (i + 1)], 0.0
+            )
+
+    def joined():
+        values = jnp.where(lane_of < head, 0.0, new_weight.astype(bf16).astype(f32) * new_rows)
+        for f, v in zip(shrink, found):
+            values = values + f * v
+        return values + pltpu.roll(values, head, 1)
 
     quads = batch // 4
+    last = len(SEGMENTS) - 1
+    for segment in range(last):
+        for q in range(quads):
+            weigh(segment, q)
     for q in range(0, MID):
-        values = weigh(values, q, 1)
+        weigh(last, q)
 
     diagonal = iota((rows, 128), 0) == lane_of
 
@@ -330,7 +353,7 @@
 
 
     for q in range(MID, quads // 2):
-        values = weigh(values, q, 1)
+        weigh(last, q)
 
     half_lane = iota((half, 128), 1)
 
@@ -341,16 +364,13 @@
             found.append(jnp.where(half_lane < head, column[low : low + half], column[high : high + half]))
         return jnp.concatenate(found, axis=0)
 
-    def fold(values):
-        return values + pltpu.roll(values, head, 1)
-
-    val_x[0, kv_index] = paired(fold(values), 0).astype(bf16)
+    val_x[0, kv_index] = paired(joined(), 0).astype(bf16)
     for q in range(quads // 2, SEND):
-        values = weigh(values, q, 1)
+        weigh(last, q)
     val_all = [exchange(val_x.at[0], (kv_index, kv_offsets))]
     for q in range(SEND, quads):
-        values = weigh(values, q, 1)
-    val_x[1, kv_index] = paired(fold(values), 1).astype(bf16)
+        weigh(last, q)
+    val_x[1, kv_index] = paired(joined(), 1).astype(bf16)
     val_all.append(exchange(val_x.at[1], (kv_index, kv_offsets)))
 
     wo_load.wait()

time: 27.3 us -> 27.1 us (level)
  no operation moved by 1% of the time
where the time goes in v6:
time: 27.1 us; the launch traced here: 27 us
  Pallas kernels  26.4 us (97%)
  between operations  0.64 us (2%)
    pallas_call x1, Pallas kernels, shards(): pl.pallas_call(functools.partial(kernel, n_kv0, n_kv1, n_tp), out_shape=(...  25.7 us
    pallas_call x1, Pallas kernels, shards(): pl.pallas_call(store, out_shape=(jax.ShapeDtypeStruct(mixed.shape, bf16),...  0.63 us

profile of v6, /device:TPU:1, one launch (start us, length us, event | category | flops | bytes accessed | tf_op | source)
XLA Modules:
  0.0 27.0 jit_solution(903105703726640272)
XLA Ops:
  0.6 25.7 %shard_map.122 = (bf16[32,256]{1,0:T(8,128)(2,1)S(1)}, f32[4,32]{1,0:T(4,128)S(1)}) custom-call(bf16[32,256]{1,0:T(8,128)(2,1)} %tokens.1, f32[1,256]{1,0:T(1,128)} %bitcast.10, bf16[256,256]{1,0:T(8,128)(2,1)} %w_query.1, bf16[64,256]{1,0:T(8,128)(2,1)} %bitcast.8, bf16[64,256]{1,0:T(8,128)(2,1)} %bitcast.9, bf16[32,4096]{1,0:T(8,128)(2,1)} %bitcast.7, ...), custom_call_target="tpu_custom_call" | custom-call | tf_op jit(solution)/shard_map/pallas_call | solution.py:431
  26.4 0.6 %shard_map.123 = (bf16[32,256]{1,0:T(8,128)(2,1)}, f32[4,32]{1,0:T(4,128)}) custom-call(bf16[32,256]{1,0:T(8,128)(2,1)S(1)} %get-tuple-element.6.mixed, f32[4,32]{1,0:T(4,128)S(1)} %get-tuple-element.7.log_weight), custom_call_target="tpu_custom_call" | custom-call | tf_op jit(solution)/shard_map/pallas_call | solution.py:483

commit v7 on v6

--- a/solution.py
+++ b/solution.py
@@ -70,8 +70,6 @@
     weights,
     query_1,
     query_2,
-    new_1,
-    new_2,
     val_x,
     stat_x,
     scale,
@@ -120,18 +118,18 @@
     small += [load(0, mine, wg_v.at[pl.ds(0, n_gates)])]
     small_new = [load(1, w_key, wkv_v.at[pl.ds(0, head)]), load(1, w_value, wkv_v.at[pl.ds(head, head)])]
 
-    scalar_loads = [load(2, lengths, len_s), load(2, gate_bias, bias_s)]
-    cum_load = load(3, cum, cum_v)
+    scalar_loads = [load(1, lengths, len_s), load(1, gate_bias, bias_s)]
+    cum_load = load(2, cum, cum_v)
+    wo_load = load(2, w_out, wo_v)
     blocks = 4
     block = batch // blocks
 
     def cache_copy(k):
         part = pl.ds(k * block, block)
-        return pltpu.make_async_copy(cache.at[part], cache_v.at[part], load_sem.at[5 + k])
+        return pltpu.make_async_copy(cache.at[part], cache_v.at[part], load_sem.at[3 + k])
 
     for k in range(blocks):
         cache_copy(k).start()
-    wo_load = load(4, w_out, wo_v)
 
     numbers = itertools.count()
     sent = []
@@ -145,7 +143,7 @@
                 pltpu.make_async_remote_copy(
                     src_ref=buffer.at[me],
                     dst_ref=buffer.at[me],
-                    send_sem=send_sem.at[number],
+                    send_sem=send_sem.at[0],
                     recv_sem=recv_sem.at[number],
                     device_id=peer(offset),
                     device_id_type=MESH,
@@ -154,7 +152,7 @@
         every = pltpu.make_async_remote_copy(
             src_ref=others,
             dst_ref=others,
-            send_sem=send_sem.at[number],
+            send_sem=send_sem.at[0],
             recv_sem=recv_sem.at[number],
             device_id=peer(ways[0][1][0]),
             device_id_type=MESH,
@@ -184,23 +182,20 @@
     part_query = jnp.dot(normed, wq_v[...], preferred_element_type=f32).astype(bf16)
     part_gate = lax.dot_general(normed, wg_v[...], NT, preferred_element_type=f32)
     part_gate = jnp.where(lane < n_gates, part_gate, squares).astype(bf16)
+    for copy in small_new + scalar_loads:
+        copy.wait()
+    part_new = lax.dot_general(normed, wkv_v[...], NT, preferred_element_type=f32).astype(bf16)
+    new_at = heads * head + 128
     for part in range(2):
         chunk = slice(part * half, (part + 1) * half)
+        query_1[first_slots[part], :, new_at:] = part_new[chunk]
         query_1[first_slots[part], :, : heads * head] = part_query[chunk]
-        query_1[first_slots[part], :, heads * head :] = part_gate[chunk]
+        query_1[first_slots[part], :, heads * head : new_at] = part_gate[chunk]
 
     pl.semaphore_wait(barrier, len(near_offsets))
     query_all = exchange(query_1, *first_ways)
-    for copy in small_new:
-        copy.wait()
-    part_new = lax.dot_general(normed, wkv_v[...], NT, preferred_element_type=f32).astype(bf16)
-    for part in range(2):
-        new_1[first_slots[part]] = part_new[part * half : (part + 1) * half]
-    new_all = exchange(new_1, *first_ways)
-
-    for copy in scalar_loads:
-        copy.wait()
     cum_load.wait()
+    wo_load.wait()
     first_pos = kv_index * span
     length_rows = jnp.zeros((batch, 128), jnp.int32)
     for b in range(batch):
@@ -245,19 +240,14 @@
     query_2[second_slots[0]] = total(query_1, 0, n_kv1).astype(bf16)
     query_2[second_slots[1]] = total(query_1, n_kv1, n_kv1 + n_kv0).astype(bf16)
     query_all = exchange(query_2, *second_ways)
-    new_all.wait_recv()
-    new_2[second_slots[0]] = total(new_1, 0, n_kv1).astype(bf16)
-    new_2[second_slots[1]] = total(new_1, n_kv1, n_kv1 + n_kv0).astype(bf16)
-    new_all = exchange(new_2, *second_ways)
     for k in range(EARLY, blocks):
         prepare(k)
     query_all.wait_recv()
-    new_all.wait_recv()
     sums = jnp.concatenate([total(query_2, 0, n_kv0), total(query_2, n_kv0, n_kv0 + n_kv1)], axis=0)
-    sum_query, gates = sums[:, : heads * head], sums[:, heads * head :]
+    sum_query, gates, sum_new = sums[:, : heads * head], sums[:, heads * head : new_at], sums[:, new_at:]
     total_squares = gates[:, n_gates : n_gates + 1]
     row_scale = lax.rsqrt(total_squares / width + norm_eps)
-    query = (row_scale * sum_query).astype(bf16).astype(f32)
+    query = sum_query.astype(bf16).astype(f32)
     log_gate = []
     for h in range(heads):
         pick = at[2] * heads + h
@@ -277,7 +267,8 @@
     lane_of = iota((rows, 128), 1)
     side = jnp.where(lane_of < head, 0, 1)
     inv_root = head ** (-0.5)
-    scaled = doubled * inv_root
+    scaled = doubled
+    row_factor = jnp.concatenate([row_scale] * heads, axis=0) * inv_root
     spread = jnp.concatenate(
         [jnp.where(row_of == 2 * p + side, scaled, 0.0).astype(bf16) for p in range(batch // 2)], axis=1
     )
@@ -286,7 +277,7 @@
     for low, high in SEGMENTS:
         top = jnp.full((rows, 128), masked_floor, f32)
         for cut in cuts(low, high):
-            score = jnp.dot(spread, keys_t[:, cut], preferred_element_type=f32) + cum_neg[:, cut]
+            score = jnp.dot(spread, keys_t[:, cut], preferred_element_type=f32) * row_factor + cum_neg[:, cut]
             biased[:, cut] = score
             for k in range(score.shape[1] // 128):
                 top = jnp.maximum(top, score[:, k * 128 : (k + 1) * 128])
@@ -299,11 +290,11 @@
         peaks.append(top)
         sums.append(jnp.sum(part_sum, axis=1, keepdims=True))
 
-    new_rows = jnp.concatenate([total(new_2, 0, n_kv0), total(new_2, n_kv0, n_kv0 + n_kv1)], axis=0)
+    new_rows = sum_new
     new_rows = (row_scale * new_rows).astype(bf16).astype(f32)
     new_rows = jnp.concatenate([new_rows] * heads, axis=0)
     new_biased = (
-        jnp.sum(jnp.where(lane_of < head, doubled * new_rows, 0.0), axis=1, keepdims=True) * inv_root
+        jnp.sum(jnp.where(lane_of < head, doubled * new_rows, 0.0), axis=1, keepdims=True) * row_factor
         - cum_query
     )
 
@@ -373,7 +364,6 @@
     val_x[1, kv_index] = paired(joined(), 1).astype(bf16)
     val_all.append(exchange(val_x.at[1], (kv_index, kv_offsets)))
 
-    wo_load.wait()
     stat_all.wait_recv()
     peaks = stat_x[:, 0, :]
     peak = jnp.max(peaks, axis=0, keepdims=True)
@@ -383,11 +373,10 @@
     factors = factors / weight_sum
     log_weight[...] = jnp.concatenate([logs[:, h * batch : (h + 1) * batch] for h in range(heads)], axis=0)
     columns = factors.T
+    out_all = []
     for part in range(2):
         for k in range(n_kv):
             scale[part, k] = paired(columns[:, k : k + 1], part)
-    out_all = []
-    for part in range(2):
         val_all[part].wait_recv()
         acc = val_x[part, 0].astype(f32) * scale[part, 0]
         for k in range(1, n_kv):
@@ -452,17 +441,15 @@
             pltpu.VMEM((rows, span), f32),
             pltpu.VMEM((rows, span), f32),
             pltpu.VMEM((rows, span), bf16),
-            pltpu.VMEM((n_kv0 + n_kv1, half, heads * head + 128), bf16),
-            pltpu.VMEM((n_kv0 + n_kv1, half, heads * head + 128), bf16),
-            pltpu.VMEM((n_kv0 + n_kv1, half, 2 * head), bf16),
-            pltpu.VMEM((n_kv0 + n_kv1, half, 2 * head), bf16),
+            pltpu.VMEM((n_kv0 + n_kv1, half, heads * head + 128 + 2 * head), bf16),
+            pltpu.VMEM((n_kv0 + n_kv1, half, heads * head + 128 + 2 * head), bf16),
             pltpu.VMEM((2, n_kv, rows // 4, 2 * head), bf16),
             pltpu.VMEM((n_kv, 4, rows), f32),
             pltpu.VMEM((2, n_kv, rows // 4, 2 * head), f32),
             pltpu.VMEM((2, n_tp, half, w_out.shape[1]), bf16),
-            pltpu.SemaphoreType.DMA((9,)),
-            pltpu.SemaphoreType.DMA((9,)),
-            pltpu.SemaphoreType.DMA((9,)),
+            pltpu.SemaphoreType.DMA((7,)),
+            pltpu.SemaphoreType.DMA((1,)),
+            pltpu.SemaphoreType.DMA((7,)),
         ],
         compiler_params=pltpu.CompilerParams(
             collective_id=0, has_side_effects=True, vmem_limit_bytes=60 * 1024 * 1024

time: 27.1 us -> 26.9 us (level)
  no operation moved by 1% of the time
where the time goes in v7:
time: 26.9 us; the launch traced here: 26.8 us
  Pallas kernels  26.2 us (97%)
  between operations  0.64 us (2%)
    pallas_call x1, Pallas kernels, shards(): pl.pallas_call(functools.partial(kernel, n_kv0, n_kv1, n_tp), out_shape=(...  25.5 us
    pallas_call x1, Pallas kernels, shards(): pl.pallas_call(store, out_shape=(jax.ShapeDtypeStruct(mixed.shape, bf16),...  0.63 us

profile of v7, /device:TPU:1, one launch (start us, length us, event | category | flops | bytes accessed | tf_op | source)
XLA Modules:
  0.0 26.8 jit_solution(12847205918980665903)
XLA Ops:
  0.6 25.5 %shard_map.122 = (bf16[32,256]{1,0:T(8,128)(2,1)S(1)}, f32[4,32]{1,0:T(4,128)S(1)}) custom-call(bf16[32,256]{1,0:T(8,128)(2,1)} %tokens.1, f32[1,256]{1,0:T(1,128)} %bitcast.10, bf16[256,256]{1,0:T(8,128)(2,1)} %w_query.1, bf16[64,256]{1,0:T(8,128)(2,1)} %bitcast.8, bf16[64,256]{1,0:T(8,128)(2,1)} %bitcast.9, bf16[32,4096]{1,0:T(8,128)(2,1)} %bitcast.7, ...), custom_call_target="tpu_custom_call" | custom-call | tf_op jit(solution)/shard_map/pallas_call | solution.py:420
  26.2 0.6 %shard_map.123 = (bf16[32,256]{1,0:T(8,128)(2,1)}, f32[4,32]{1,0:T(4,128)}) custom-call(bf16[32,256]{1,0:T(8,128)(2,1)S(1)} %get-tuple-element.6.mixed, f32[4,32]{1,0:T(4,128)S(1)} %get-tuple-element.7.log_weight), custom_call_target="tpu_custom_call" | custom-call | tf_op jit(solution)/shard_map/pallas_call | solution.py:470
